TPU v7x, 128 devices: a whole 4x4x4 slice. The times are simulated.
128 devices in a mesh: sp: 16 (over z, x), dp: 8 (over y, core).
Axes of the slice: x: 4, y: 4, z: 4, core: 2. Of those that a mesh axis runs over, the one named last changes fastest.
Arguments:
- resid: bfloat16 [8, 4096, 2048], P('dp', 'sp'), may hold values from -4 to 4
- query: bfloat16 [8, 4096, 2048], P('dp', 'sp'), may hold values from -6 to 6
- keys: bfloat16 [8, 4096, 512], P('dp', 'sp'), may hold values from -6 to 6
- values: bfloat16 [8, 4096, 512], P('dp', 'sp'), may hold values from -6 to 6
- q_gain: float32 [128], replicated, may hold values from 0.7 to 5
- k_gain: float32 [128], replicated, may hold values from 0.7 to 5
- out_weight: bfloat16 [2048, 2048], P('dp'), may hold values from -0.5 to 0.5
- norm_gain: float32 [2048], replicated, may hold values from 0.1 to 1.9
- route_ids: int32 [8, 4096, 2], P('dp', 'sp'), may hold values from 0 to 127, all different within a row; in each aligned block of 256 rows (0 to 255, 256 to 511, ..., all dimensions but the last counted through in order) at most 6 rows name the same one
- route_weight: float32 [8, 4096, 2], P('dp', 'sp'), may hold values from 0.2 to 1
- expert_gate: bfloat16 [128, 2048, 1024], P(('sp', 'dp')), may hold values from -0.125 to 0.125
- expert_up: bfloat16 [128, 2048, 1024], P(('sp', 'dp')), may hold values from -0.125 to 0.125
- expert_down: bfloat16 [128, 1024, 2048], P(('sp', 'dp')), may hold values from -0.1875 to 0.1875
Outputs:
- layer_out: bfloat16 [8, 4096, 2048], P('dp', 'sp')
Inputs may be any that keep to these rules, and one draw needn't show every extreme that they name: `route_ids`: each row names 2 different experts. In the rows of one device no expert is named more than 6 times, and in some devices some expert is named exactly 6 times.
All inputs are finite; a program needn't handle non-finite values.
Results may differ from a plain program's by a relative error of at most 0.0095.
The roundings to bfloat16 on the way count: a program that leaves them out, or rounds other values in their place, can miss the bound.
Values may be sent and summed in bfloat16 or wider, within the bound.
A program may use at most 128 MiB of HBM per device.

v0:
```python
import jax
import jax.numpy as jnp
from jax import lax
from jax.sharding import PartitionSpec as P

GRID_W = 64


EPSILON = 1e-06
THETA = 10000.0
LIMIT = 7.0
SLOPE = 1.702


def turn_half(matrix, places):
    half_width = matrix.shape[-1] // 2
    inverse = THETA ** (-jnp.arange(half_width, dtype=jnp.float32) / half_width)
    angles = places.astype(jnp.float32)[:, None] * inverse[None, :]
    cosine = jnp.cos(angles)[:, None, :]
    sine_part = jnp.sin(angles)[:, None, :]
    leading = matrix[..., :half_width]
    second = matrix[..., half_width:]
    return jnp.concatenate(
        [leading * cosine - second * sine_part, second * cosine + leading * sine_part], axis=-1
    )


def prepare(projected_rows, gain_vector, head_count, places):
    matrix = projected_rows.astype(jnp.float32).reshape(projected_rows.shape[0], head_count, -1)
    matrix = (
        matrix
        * lax.rsqrt(jnp.mean(matrix * matrix, axis=-1, keepdims=True) + EPSILON)
        * gain_vector
    )
    middle = matrix.shape[-1] // 2
    turned = jnp.concatenate(
        [
            turn_half(matrix[..., :middle], places // GRID_W),
            turn_half(matrix[..., middle:], places % GRID_W),
        ],
        axis=-1,
    )
    return turned.astype(jnp.bfloat16)


def attend(head_query, head_key, head_value):
    length, local_heads, head_dim = head_query.shape
    local_kv = head_key.shape[1]
    group_size = local_heads // local_kv
    block_rows = min(512, length)
    scaling = head_dim ** (-0.5)
    query_blocks = head_query.reshape(
        length // block_rows, block_rows, local_kv, group_size, head_dim
    )

    def one_block(query_block):
        scores = (
            jnp.einsum("qkgd,skd->kgqs", query_block, head_key, preferred_element_type=jnp.float32)
            * scaling
        )
        lifted = jnp.exp(scores - jnp.max(scores, axis=-1, keepdims=True))
        attn_weights = (lifted / jnp.sum(lifted, axis=-1, keepdims=True)).astype(jnp.bfloat16)
        return jnp.einsum(
            "kgqs,skd->qkgd", attn_weights, head_value, preferred_element_type=jnp.float32
        ).astype(jnp.bfloat16)

    return lax.map(one_block, query_blocks).reshape(length, local_heads, head_dim)


def apply_expert(batch, gate_matrix, up_matrix, down_matrix):
    flat_rows = batch.reshape(-1, batch.shape[-1])
    gated = jnp.minimum(jnp.dot(flat_rows, gate_matrix, preferred_element_type=jnp.float32), LIMIT)
    linear = jnp.clip(
        jnp.dot(flat_rows, up_matrix, preferred_element_type=jnp.float32), -LIMIT, LIMIT
    )
    active = (gated * jax.nn.sigmoid(SLOPE * gated) * (linear + 1.0)).astype(jnp.bfloat16)
    return (
        jnp.dot(active, down_matrix, preferred_element_type=jnp.float32)
        .astype(jnp.bfloat16)
        .reshape(batch.shape)
    )


def per_device(
    resid,
    query,
    keys,
    values,
    q_gain,
    k_gain,
    out_weight,
    norm_gain,
    route_ids,
    route_weight,
    expert_gate,
    expert_up,
    expert_down,
):
    span_devices = lax.axis_size("sp")
    experts_total = span_devices * lax.axis_size("dp")
    tok_rows = resid.shape[1]
    model_width = resid.shape[2]
    head_dim = q_gain.shape[0]
    q_heads = query.shape[2] // head_dim
    kv_heads = keys.shape[2] // head_dim
    repeat_count = max(kv_heads, span_devices) // kv_heads
    places = lax.axis_index("sp") * tok_rows + jnp.arange(tok_rows, dtype=jnp.int32)
    query_turned = prepare(query[0], q_gain, q_heads, places)
    key_turned = jnp.repeat(prepare(keys[0], k_gain, kv_heads, places), repeat_count, axis=1)
    value_heads = jnp.repeat(values[0].reshape(tok_rows, kv_heads, head_dim), repeat_count, axis=1)
    head_query, head_key, head_value = (
        lax.all_to_all(query_turned, "sp", split_axis=1, concat_axis=0, tiled=True),
        lax.all_to_all(key_turned, "sp", split_axis=1, concat_axis=0, tiled=True),
        lax.all_to_all(value_heads, "sp", split_axis=1, concat_axis=0, tiled=True),
    )
    head_out = attend(head_query, head_key, head_value)
    token_out = lax.all_to_all(head_out, "sp", split_axis=0, concat_axis=1, tiled=True).reshape(
        tok_rows, q_heads * head_dim
    )
    projected = jnp.dot(
        token_out,
        lax.all_gather(out_weight, "dp", axis=0, tiled=True),
        preferred_element_type=jnp.float32,
    )
    updated = (resid[0].astype(jnp.float32) + projected).astype(jnp.bfloat16)
    widened = updated.astype(jnp.float32)
    normed = (
        widened
        * lax.rsqrt(jnp.mean(widened * widened, axis=-1, keepdims=True) + EPSILON)
        * norm_gain
    ).astype(jnp.bfloat16)
    top_count = route_ids.shape[2]
    capacity = max(2, 3 * tok_rows * top_count // (2 * experts_total))
    chosen = route_ids[0].reshape(-1)
    onehot = (chosen[:, None] == jnp.arange(experts_total, dtype=jnp.int32)[None, :]).astype(
        jnp.int32
    )
    earlier = jnp.sum((jnp.cumsum(onehot, axis=0) - onehot) * onehot, axis=1)
    target = chosen * capacity + earlier
    sources = jnp.arange(tok_rows * top_count, dtype=jnp.int32) // top_count
    slot_table = jnp.full((experts_total * capacity,), tok_rows, jnp.int32).at[target].set(sources)
    padded = jnp.concatenate([normed, jnp.zeros((1, model_width), jnp.bfloat16)], axis=0)
    outgoing = padded[slot_table].reshape(experts_total, capacity, model_width)
    answered = apply_expert(
        lax.all_to_all(outgoing, ("sp", "dp"), split_axis=0, concat_axis=0, tiled=True),
        expert_gate[0],
        expert_up[0],
        expert_down[0],
    )
    returned = lax.all_to_all(answered, ("sp", "dp"), split_axis=0, concat_axis=0, tiled=True)
    results = returned.reshape(experts_total * capacity, model_width)[target]
    weighted = results.astype(jnp.float32) * route_weight[0].reshape(-1)[:, None]
    combined = jnp.sum(weighted.reshape(tok_rows, top_count, model_width), axis=1)
    return (widened + combined).astype(jnp.bfloat16)[None]


def solution(mesh):
    placed = (
        P("dp", "sp", None),
        P("dp", "sp", None),
        P("dp", "sp", None),
        P("dp", "sp", None),
        P(),
        P(),
        P("dp", None),
        P(),
        P("dp", "sp", None),
        P("dp", "sp", None),
        P(("sp", "dp"), None, None),
        P(("sp", "dp"), None, None),
        P(("sp", "dp"), None, None),
    )
    return jax.shard_map(
        per_device, mesh=mesh, in_specs=placed, out_specs=P("dp", "sp", None), check_vma=False
    )
```

profile of v0, /device:TPU:6, one launch (start us, length us, event | category | flops | bytes accessed | tf_op | source)
XLA Modules:
  0.0 342.8 jit_solution(1919903643799338498)
XLA Ops:
  12.8 8.3 %all-to-all-start.1 = ((bf16[256,16,128]{2,0,1:T(8,128)(2,1)}), bf16[256,16,128]{2,0,1:T(8,128)(2,1)S(1)}, u32[]{:S(2)}, u32[]{:S(2)}) async-start(bf16[256,16,128]{2,0,1:T(8,128)(2,1)} %bitcast.18), calls=%async_computation.1 | async-start | bytes 2097152 | tf_op jit(solution)/shard_map/all_to_all | solution.py:113
  23.6 12.0 %all-to-all-done.1 = bf16[256,16,128]{2,0,1:T(8,128)(2,1)S(1)} async-done(((bf16[256,16,128]{2,0,1:T(8,128)(2,1)}), bf16[256,16,128]{2,0,1:T(8,128)(2,1)S(1)}, u32[]{:S(2)}, u32[]{:S(2)}) %all-to-all-start.1) | async-done | bytes 1048608 | tf_op jit(solution)/shard_map/all_to_all | solution.py:113
  35.6 6.7 %all-to-all-start = ((bf16[256,16,128]{0,2,1:T(8,128)(2,1)}), bf16[256,16,128]{0,2,1:T(8,128)(2,1)S(1)}, u32[]{:S(2)}, u32[]{:S(2)}) async-start(bf16[256,16,128]{0,2,1:T(8,128)(2,1)} %pad_maximum_fusion), calls=%async_computation | async-start | bytes 2097152 | tf_op jit(solution)/shard_map/all_to_all | solution.py:112
  42.4 13.4 %all-to-all-done = bf16[256,16,128]{0,2,1:T(8,128)(2,1)S(1)} async-done(((bf16[256,16,128]{0,2,1:T(8,128)(2,1)}), bf16[256,16,128]{0,2,1:T(8,128)(2,1)S(1)}, u32[]{:S(2)}, u32[]{:S(2)}) %all-to-all-start) | async-done | bytes 1048608 | tf_op jit(solution)/shard_map/all_to_all | solution.py:112
  57.0 7.0 %all-to-all-start.2 = ((bf16[256,16,128]{2,0,1:T(8,128)(2,1)}), bf16[256,16,128]{2,0,1:T(8,128)(2,1)}, u32[]{:S(2)}, u32[]{:S(2)}) async-start(bf16[256,16,128]{2,0,1:T(8,128)(2,1)} %bitcast.22), calls=%async_computation.2 | async-start | bytes 2097152 | tf_op jit(solution)/shard_map/all_to_all | solution.py:114
  66.3 10.8 %all-to-all-done.2 = bf16[256,16,128]{2,0,1:T(8,128)(2,1)} async-done(((bf16[256,16,128]{2,0,1:T(8,128)(2,1)}), bf16[256,16,128]{2,0,1:T(8,128)(2,1)}, u32[]{:S(2)}, u32[]{:S(2)}) %all-to-all-start.2) | async-done | bytes 1048608 | tf_op jit(solution)/shard_map/all_to_all | solution.py:114
  77.1 52.3 %while.10 = (s32[]{:T(128)}, bf16[8,512,1,1,128]{4,1,3,2,0:T(8,128)(2,1)}, bf16[8,512,1,1,128]{4,1,3,2,0:T(8,128)(2,1)S(1)}, bf16[4096,1,128]{2,0,1:T(8,128)(2,1)S(1)}, bf16[4096,1,128]{2,0,1:T(8,128)(2,1)}, /*index=5*/s32[]{:T(128)}) while((s32[]{:T(128)}, bf16[8,512,1,1,128]{4,1,3,2,0:T(8,128)(2,1)}, ...), condition=%wide.region_5.6_spmd, body=%wide.region_2.5_spmd.sunk | while | flops 1092680704 | bytes 27535944 | solution.py:67
  80.0 3.8 %fusion.65 = bf16[8,512,1,1,128]{4,1,3,2,0:T(8,128)(2,1)} fusion(bf16[8,512,1,1,128]{4,1,3,2,0:T(8,128)(2,1)} %get-tuple-element.139, s32[]{:T(128)} %get-tuple-element.138, f32[512]{0:T(512)S(1)} %fusion.64, f32[512]{0:T(512)S(1)} %get-tuple-element.131, f32[512,4096]{1,0:T(8,128)S(1)} %get-tuple-element.130, ...), kind=kOutput, calls=%fused_computation.13.clone.1 | convolution fusion | flops 545325056 | bytes 9572864 | tf_op jit(solution)/shard_map/while/body/eval_jaxpr/kgqs,skd->qkgd/dot_general | solution.py:63
  86.6 3.7 %fusion.65 = bf16[8,512,1,1,128]{4,1,3,2,0:T(8,128)(2,1)} fusion(bf16[8,512,1,1,128]{4,1,3,2,0:T(8,128)(2,1)} %get-tuple-element.139, s32[]{:T(128)} %get-tuple-element.138, f32[512]{0:T(512)S(1)} %fusion.64, f32[512]{0:T(512)S(1)} %get-tuple-element.131, f32[512,4096]{1,0:T(8,128)S(1)} %get-tuple-element.130, ...), kind=kOutput, calls=%fused_computation.13.clone.1 | convolution fusion | flops 545325056 | bytes 9572864 | tf_op jit(solution)/shard_map/while/body/eval_jaxpr/kgqs,skd->qkgd/dot_general | solution.py:63
  99.6 3.8 %fusion.65 = bf16[8,512,1,1,128]{4,1,3,2,0:T(8,128)(2,1)} fusion(bf16[8,512,1,1,128]{4,1,3,2,0:T(8,128)(2,1)} %get-tuple-element.139, s32[]{:T(128)} %get-tuple-element.138, f32[512]{0:T(512)S(1)} %fusion.64, f32[512]{0:T(512)S(1)} %get-tuple-element.131, f32[512,4096]{1,0:T(8,128)S(1)} %get-tuple-element.130, ...), kind=kOutput, calls=%fused_computation.13.clone.1 | convolution fusion | flops 545325056 | bytes 9572864 | tf_op jit(solution)/shard_map/while/body/eval_jaxpr/kgqs,skd->qkgd/dot_general | solution.py:63
  133.6 6.4 %all-to-all-start.3 = ((bf16[16,2,16384]{2,1,0:T(2,128)(2,1)}), bf16[16,2,16384]{2,1,0:T(2,128)(2,1)S(1)}, u32[]{:S(2)}, u32[]{:S(2)}) async-start(bf16[16,2,16384]{2,1,0:T(2,128)(2,1)} %reshape.324), calls=%async_computation.3 | async-start | bytes 2097152 | tf_op jit(solution)/shard_map/all_to_all | solution.py:117
  143.0 9.5 %all-to-all-done.3 = bf16[16,2,16384]{2,1,0:T(2,128)(2,1)S(1)} async-done(((bf16[16,2,16384]{2,1,0:T(2,128)(2,1)}), bf16[16,2,16384]{2,1,0:T(2,128)(2,1)S(1)}, u32[]{:S(2)}, u32[]{:S(2)}) %all-to-all-start.3) | async-done | bytes 1048608 | tf_op jit(solution)/shard_map/all_to_all | solution.py:117
  154.3 6.1 %fusion.33 = (f32[256]{0:T(256)S(1)}, bf16[256,2048]{1,0:T(8,128)(2,1)S(1)}) fusion(bf16[256,2048]{0,1:T(8,128)(2,1)S(1)} %bitcast.134, bf16[2048,2048]{1,0:T(8,128)(2,1)} %all-gather.2.cloned.1.call-done, bf16[1,256,2048]{2,1,0:T(8,128)(2,1)} %param.15), kind=kOutput, calls=%fused_computation.39 | convolution fusion | flops 2150629120 | bytes 11535360 | tf_op jit(solution)/shard_map/dot_general | solution.py:120
  161.7 4.3 %gather_fusion = bf16[768,2048]{1,0:T(8,128)(2,1)} fusion(bf16[257,2048]{1,0:T(8,128)(2,1)S(1)} %concatenate.13, s32[1024]{0:T(1024)S(1)} %pad_clamp_fusion.1), kind=kCustom, calls=%fused_computation | custom fusion | bytes 6294528 | tf_op jit(solution)/shard_map/gather | solution.py:143
  166.0 6.3 %reshape.289 = bf16[128,6,2048]{2,1,0:T(8,128)(2,1)} reshape(bf16[768,2048]{1,0:T(8,128)(2,1)} %gather_fusion) | data formatting | bytes 6291456 | tf_op jit(solution)/shard_map/reshape | solution.py:143
  172.3 60.4 %all_to_all.76 = bf16[128,6,2048]{2,1,0:T(8,128)(2,1)} all-to-all(bf16[128,6,2048]{2,1,0:T(8,128)(2,1)} %reshape.289), channel_id=1, replica_groups=mesh['sp'=16,'dp'=8] {'sp','dp'}, dimensions={0} | all-to-all | bytes 6291456 | tf_op jit(solution)/shard_map/all_to_all | solution.py:145
  232.7 4.9 %reshape.290 = bf16[768,2048]{1,0:T(8,128)(2,1)S(1)} reshape(bf16[128,6,2048]{2,1,0:T(8,128)(2,1)} %all_to_all.76) | data formatting | bytes 6291456 | tf_op jit(solution)/shard_map/reshape | solution.py:71
  237.6 5.3 %fusion.23 = f32[768,1024]{1,0:T(8,128)S(1)} fusion(bf16[768,2048]{1,0:T(8,128)(2,1)S(1)} %reshape.290, bf16[1,2048,1024]{2,1,0:T(8,128)(2,1)} %param.26), kind=kOutput, calls=%fused_computation.23 | convolution fusion | flops 3221225472 | bytes 10485760 | tf_op jit(solution)/shard_map/dot_general | solution.py:74
  242.9 4.1 %multiply_convert_fusion = bf16[768,1024]{1,0:T(8,128)(2,1)S(1)} fusion(f32[768,1024]{1,0:T(8,128)S(1)} %fusion.23, bf16[768,2048]{1,0:T(8,128)(2,1)S(1)} %reshape.290, bf16[1,2048,1024]{2,1,0:T(8,128)(2,1)S(1)} %copy-done.8), kind=kOutput, calls=%fused_computation.29 | convolution fusion | flops 3229089792 | bytes 12058624 | tf_op jit(solution)/shard_map/dot_general | solution.py:72
  253.6 6.8 %all-to-all-start.5 = ((bf16[128,6,2048]{2,1,0:T(8,128)(2,1)}), bf16[128,6,2048]{2,1,0:T(8,128)(2,1)}, u32[]{:S(2)}, u32[]{:S(2)}) async-start(bf16[128,6,2048]{2,1,0:T(8,128)(2,1)} %reshape.291), calls=%async_computation.5 | async-start | bytes 8388608 | tf_op jit(solution)/shard_map/all_to_all | solution.py:150
  260.6 51.5 %all-to-all-done.5 = bf16[128,6,2048]{2,1,0:T(8,128)(2,1)} async-done(((bf16[128,6,2048]{2,1,0:T(8,128)(2,1)}), bf16[128,6,2048]{2,1,0:T(8,128)(2,1)}, u32[]{:S(2)}, u32[]{:S(2)}) %all-to-all-start.5) | async-done | bytes 3145760 | tf_op jit(solution)/shard_map/all_to_all | solution.py:150
  312.1 4.9 %reshape.292 = bf16[768,2048]{1,0:T(8,128)(2,1)S(1)} reshape(bf16[128,6,2048]{2,1,0:T(8,128)(2,1)} %all-to-all-done.5) | data formatting | bytes 6291456 | tf_op jit(solution)/shard_map/reshape | solution.py:151
  320.3 5.4 %reshape.296 = f32[256,2,2048]{2,1,0:T(2,128)} reshape(bf16[512,2048]{1,0:T(8,128)(2,1)} %gather_fusion.1) | data formatting | bytes 6291456 | tf_op jit(solution)/shard_map/convert_element_type | solution.py:152
  325.7 9.0 %multiply_reduce_fusion.1 = f32[256,2048]{1,0:T(8,128)S(1)} fusion(f32[256,2,2048]{2,1,0:T(2,128)} %reshape.296, f32[256,2]{1,0:T(8,128)S(1)} %copy.112), kind=kLoop, calls=%fused_computation.27 | loop fusion | flops 1572864 | bytes 6293504 | tf_op jit(solution)/shard_map/reduce_sum | solution.py:153
  (105 shorter events, 74.7 us)
Async XLA Ops:
  10.7 10.3 %copy-start.2 = (bf16[1,256,2048]{2,1,0:T(8,128)(2,1)S(1)}, bf16[1,256,2048]{2,1,0:T(8,128)(2,1)}, u32[]{:S(2)}) copy-start(bf16[1,256,2048]{2,1,0:T(8,128)(2,1)} %param.16) | copy-start | bytes 3145732
  11.6 10.3 %copy-start.7 = (f32[128]{0:T(128)S(1)}, f32[128]{0:T(128)}, u32[]{:S(2)}) copy-start(f32[128]{0:T(128)} %param.19) | copy-start | bytes 1540
  12.8 22.8 %all-to-all-start.1 = ((bf16[256,16,128]{2,0,1:T(8,128)(2,1)}), bf16[256,16,128]{2,0,1:T(8,128)(2,1)S(1)}, u32[]{:S(2)}, u32[]{:S(2)}) async-start(bf16[256,16,128]{2,0,1:T(8,128)(2,1)} %bitcast.18), calls=%async_computation.1 | async-start | bytes 2097152 | tf_op jit(solution)/shard_map/all_to_all | solution.py:113
  22.2 20.1 %copy-start.3 = (bf16[1,256,512]{2,1,0:T(8,128)(2,1)S(1)}, bf16[1,256,512]{2,1,0:T(8,128)(2,1)}, u32[]{:S(2)}) copy-start(bf16[1,256,512]{2,1,0:T(8,128)(2,1)} %param.18) | copy-start | bytes 786436
  35.6 20.2 %all-to-all-start = ((bf16[256,16,128]{0,2,1:T(8,128)(2,1)}), bf16[256,16,128]{0,2,1:T(8,128)(2,1)S(1)}, u32[]{:S(2)}, u32[]{:S(2)}) async-start(bf16[256,16,128]{0,2,1:T(8,128)(2,1)} %pad_maximum_fusion), calls=%async_computation | async-start | bytes 2097152 | tf_op jit(solution)/shard_map/all_to_all | solution.py:112
  42.3 22.5 %copy-start.5 = (s32[1,256,2]{1,2,0:T(2,128)S(1)}, s32[1,256,2]{1,2,0:T(2,128)}, u32[]{:S(2)}) copy-start(s32[1,256,2]{1,2,0:T(2,128)} %param.23) | copy-start | bytes 6148
  57.0 20.1 %all-to-all-start.2 = ((bf16[256,16,128]{2,0,1:T(8,128)(2,1)}), bf16[256,16,128]{2,0,1:T(8,128)(2,1)}, u32[]{:S(2)}, u32[]{:S(2)}) async-start(bf16[256,16,128]{2,0,1:T(8,128)(2,1)} %bitcast.22), calls=%async_computation.2 | async-start | bytes 2097152 | tf_op jit(solution)/shard_map/all_to_all | solution.py:114
  64.1 90.2 %all-gather.2.cloned.1.call-start = ((), (), s32[]{:S(2)}) async-start(), calls=%async_computation.6 | async-start | bytes 9437184 | tf_op jit(solution)/shard_map/all_gather | solution.py:122
  133.6 18.9 %all-to-all-start.3 = ((bf16[16,2,16384]{2,1,0:T(2,128)(2,1)}), bf16[16,2,16384]{2,1,0:T(2,128)(2,1)S(1)}, u32[]{:S(2)}, u32[]{:S(2)}) async-start(bf16[16,2,16384]{2,1,0:T(2,128)(2,1)} %reshape.324), calls=%async_computation.3 | async-start | bytes 2097152 | tf_op jit(solution)/shard_map/all_to_all | solution.py:117
  154.3 7.1 %copy-start.4 = (f32[2048]{0:T(1024)S(1)}, f32[2048]{0:T(1024)}, u32[]{:S(2)}) copy-start(f32[2048]{0:T(1024)} %param.22) | copy-start | bytes 24580
  160.4 1.0 copy-start
  237.6 5.4 %copy-start.8 = (bf16[1,2048,1024]{2,1,0:T(8,128)(2,1)S(1)}, bf16[1,2048,1024]{2,1,0:T(8,128)(2,1)}, u32[]{:S(2)}) copy-start(bf16[1,2048,1024]{2,1,0:T(8,128)(2,1)} %param.25) | copy-start | bytes 12582916
  242.9 4.2 %copy-start.9 = (bf16[1,1024,2048]{2,1,0:T(8,128)(2,1)S(1)}, bf16[1,1024,2048]{2,1,0:T(8,128)(2,1)}, u32[]{:S(2)}) copy-start(bf16[1,1024,2048]{2,1,0:T(8,128)(2,1)} %param.27) | copy-start | bytes 12582916
  253.6 6.8 %copy-start.6 = (f32[1,256,2]{1,2,0:T(2,128)S(1)}, f32[1,256,2]{1,2,0:T(2,128)}, u32[]{:S(2)}) copy-start(f32[1,256,2]{1,2,0:T(2,128)} %param.24) | copy-start | bytes 6148
  253.6 58.5 %all-to-all-start.5 = ((bf16[128,6,2048]{2,1,0:T(8,128)(2,1)}), bf16[128,6,2048]{2,1,0:T(8,128)(2,1)}, u32[]{:S(2)}, u32[]{:S(2)}) async-start(bf16[128,6,2048]{2,1,0:T(8,128)(2,1)} %reshape.291), calls=%async_computation.5 | async-start | bytes 8388608 | tf_op jit(solution)/shard_map/all_to_all | solution.py:150
  325.7 9.0 %copy-start.1 = (bf16[256,2048]{1,0:T(8,128)(2,1)S(1)}, bf16[256,2048]{1,0:T(8,128)(2,1)}, u32[]{:S(2)}) copy-start(bf16[256,2048]{1,0:T(8,128)(2,1)} %copy-done) | copy-start | bytes 3145732
Sparse Core Ops, SparseCore 0:
  66.6 50.9 all-gather.1
where the time goes:
time: 346 us; the launch traced here: 343 us
  waiting for transfers between devices  97.9 us (28%)
  blocking collectives  60.4 us (17%)
  matrix products  59.4 us (17%)
  local copies, waits for them, and re-layouts  44.9 us (13%)
  starting transfers between devices  35.2 us (10%)
  other arithmetic  31.1 us (9%)
  between operations  13.9 us (4%)
    all_to_all x1, blocking collectives, per_device(): lax.all_to_all(outgoing, ('sp', 'dp'), split_axis=0, concat_axis=0, tiled...  60.4 us
    all_to_all x1, waiting for transfers between devices, per_device(): lax.all_to_all(answered, ('sp', 'dp'), split_axis=0, concat_axis=0, tiled...  51.5 us
    dot_general x8, matrix products, one_block(): jnp.einsum('kgqs,skd->qkgd', attn_weights, head_value, preferred_element_...  29.6 us
    all_to_all x1, waiting for transfers between devices, per_device(): lax.all_to_all(query_turned, 'sp', split_axis=1, concat_axis=0, tiled=True)  13.4 us
    reduce_sum x8, other arithmetic, one_block(): jnp.sum(lifted, axis=-1, keepdims=True)  12 us
    all_to_all x1, waiting for transfers between devices, per_device(): lax.all_to_all(key_turned, 'sp', split_axis=1, concat_axis=0, tiled=True)  12 us
    all_to_all x1, waiting for transfers between devices, per_device(): lax.all_to_all(value_heads, 'sp', split_axis=1, concat_axis=0, tiled=True)  10.8 us
    dot_general x8, matrix products, one_block(): jnp.einsum('qkgd,skd->kgqs', query_block, head_key, preferred_element_typ...  10.6 us
  transfers between devices with their start and end apart: 6, of which 5 were waited for; matrix products, arithmetic and copies ran while one was open for 19% of the time, Pallas kernels for 0%

commit v1 on v0

v1 whole, which is shorter than its diff:
```python
import functools
import jax
import jax.numpy as jnp
from jax import lax
from jax.experimental import pallas as pl
from jax.experimental.pallas import tpu as pltpu
from jax.sharding import PartitionSpec as P

GRID_W = 64
EPSILON = 1e-06
THETA = 10000.0
LIMIT = 7.0
SLOPE = 1.702
LOG2E = 1.4426950408889634
HD = 128
TOK = 256
ZN = 4
XN = 4
N_DEV = 128
CAP = 6
BF = jnp.bfloat16
F32 = jnp.float32
MESH = pl.DeviceIdType.MESH
VM = pl.BlockSpec(memory_space=pltpu.VMEM)
SM = pl.BlockSpec(memory_space=pltpu.SMEM)
MB = 1 << 20


def params(limit=48 * MB, cid=None, **kw):
    if cid is not None:
        kw.update(collective_id=cid, has_side_effects=True)
    return pltpu.CompilerParams(vmem_limit_bytes=limit, **kw)


def turn_tables(places):
    lane = jnp.arange(HD, dtype=jnp.int32)
    inverse = THETA ** (-(lane % 32).astype(F32) / 32)
    place = jnp.where(lane[None, :] < 64, (places // GRID_W)[:, None], (places % GRID_W)[:, None])
    angles = place.astype(F32) * inverse[None, :]
    sign = jnp.where(lane % 64 < 32, -1.0, 1.0)
    return jnp.cos(angles), jnp.sin(angles) * sign[None, :]


def turn_head(x, gain, cosine, sine, first):
    x = x.astype(F32)
    x = x * lax.rsqrt(jnp.mean(x * x, axis=-1, keepdims=True) + EPSILON) * gain
    other = jnp.where(first, pltpu.roll(x, HD - 32, 1), pltpu.roll(x, 32, 1))
    return (x * cosine + other * sine).astype(BF)


def prep_kernel(q_ref, k_ref, v_ref, qg_ref, kg_ref, cos_ref, sin_ref, idr_ref, idc_ref,
                qs_ref, kvs_ref, tgt_ref, slot_ref):
    first = lax.broadcasted_iota(jnp.int32, (TOK, HD), 1) % 64 < 32
    cosine, sine = cos_ref[...], sin_ref[...]
    for h in range(16):
        qs_ref[h // 4, :, (h % 4) * HD:(h % 4 + 1) * HD] = turn_head(
            q_ref[:, h * HD:(h + 1) * HD], qg_ref[...], cosine, sine, first)
    for h in range(4):
        kvs_ref[h, 0] = turn_head(k_ref[:, h * HD:(h + 1) * HD], kg_ref[...], cosine, sine, first)
        kvs_ref[h, 1] = v_ref[:, h * HD:(h + 1) * HD]
    n = 2 * TOK
    row, col = idr_ref[...], idc_ref[...]
    ia = lax.broadcasted_iota(jnp.int32, (n, n), 0)
    ib = lax.broadcasted_iota(jnp.int32, (n, n), 1)
    same = col == row
    before = jnp.sum(jnp.where(same & (ia < ib), 1.0, 0.0), axis=0, keepdims=True)
    tgt_ref[...] = row * CAP + before.astype(jnp.int32)
    before_c = jnp.sum(jnp.where(same & (ib < ia), 1.0, 0.0), axis=1, keepdims=True)
    target = col * CAP + before_c.astype(jnp.int32)
    slots = lax.broadcasted_iota(jnp.int32, (n, N_DEV * CAP), 1)
    token = (lax.broadcasted_iota(jnp.int32, (n, N_DEV * CAP), 0) // 2).astype(F32)
    slot_ref[...] = jnp.sum(jnp.where(target == slots, token, 0.0), axis=0, keepdims=True).astype(jnp.int32)


def sp_of(z, x):
    return {"sp": lax.rem(z, ZN) * XN + lax.rem(x, XN)}


def spread_kernel(qs_ref, kvs_ref, q_ref, kv_ref, zks, zkr, zqs, zqr, xs, xr, fs, fr):
    sp = lax.axis_index("sp")
    z, x = sp // XN, lax.rem(sp, XN)
    bar = pltpu.get_barrier_semaphore()
    for d in (1, 2, 3):
        pl.semaphore_signal(bar, inc=1, device_id=sp_of(z + d, x), device_id_type=MESH)
    for d in (1, 3):
        pl.semaphore_signal(bar, inc=1, device_id=sp_of(z, x + d), device_id_type=MESH)
    pl.semaphore_wait(bar, 5)
    pending = []

    def send(src, dst, ssem, rsem, dev):
        c = pltpu.make_async_remote_copy(src, dst, ssem, rsem, device_id=dev, device_id_type=MESH)
        c.start()
        pending.append(c)
        return c

    zk = {}
    for d in (1, 3, 2):
        zk[d] = send(kvs_ref.at[lax.rem(z + d, ZN)], kv_ref.at[x, z], zks.at[d - 1], zkr.at[d - 1], sp_of(z + d, x))
    kv_ref[x, z] = kvs_ref[z]

    def gather(d):
        chunk = lax.rem(z + ZN - d, ZN)
        return [send(kv_ref.at[x, chunk], kv_ref.at[x, chunk], xs.at[s, d], xr.at[s, d], sp_of(z, x + (1, 3)[s])) for s in (0, 1)]

    near = {0: gather(0)}
    zq = {}
    for d in (1, 3, 2):
        zq[d] = send(qs_ref.at[lax.rem(z + d, ZN)], q_ref.at[z], zqs.at[d - 1], zqr.at[d - 1], sp_of(z + d, x))
    q_ref[z] = qs_ref[z]
    far = []

    def forward(d):
        chunk = lax.rem(z + ZN - d, ZN)
        s = 0 if d in (0, 1) else 1
        near[d][s].wait_recv()
        came = lax.rem(x + (3, 1)[s], XN)
        far.append(send(kv_ref.at[came, chunk], kv_ref.at[came, chunk], fs.at[d], fr.at[d], sp_of(z, x + (1, 3)[s])))

    prev = 0
    for d in (1, 3, 2):
        zk[d].wait_recv()
        near[d] = gather(d)
        forward(prev)
        prev = d
    forward(prev)
    for d in (0, 1, 2, 3):
        s = 0 if d in (0, 1) else 1
        near[d][1 - s].wait_recv()
    for d in (1, 3, 2):
        zq[d].wait_recv()
    for c in far:
        c.wait_recv()
    for c in pending:
        c.wait_send()


def attend_kernel(q_ref, kv_ref, o_ref, ve_ref):
    scale = HD ** -0.5 * LOG2E

    @pl.when(pl.program_id(0) == 0)
    def _():
        lane = lax.broadcasted_iota(jnp.int32, (1024, HD), 1)
        for c in range(4):
            ve_ref[c * 1024:(c + 1) * 1024, :HD] = kv_ref[c, :, 1].reshape(1024, HD)
            ve_ref[c * 1024:(c + 1) * 1024, HD:] = jnp.where(lane == 0, 1.0, 0.0).astype(BF)

    q = q_ref[0]
    m = acc = None
    for c in range(4):
        k = kv_ref[c, :, 0].reshape(1024, HD)
        s = lax.dot_general(q, k, (((1,), (1,)), ((), ())), preferred_element_type=F32)
        top = jnp.max(s, axis=-1, keepdims=True) * scale
        m_new = top if m is None else jnp.maximum(m, top)
        p = jnp.exp2(s * scale - m_new).astype(BF)
        part = jnp.dot(p, ve_ref[c * 1024:(c + 1) * 1024, :], preferred_element_type=F32)
        acc = part if acc is None else acc * jnp.exp2(m - m_new) + part
        m = m_new
    o_ref[0] = (acc[:, :HD] / acc[:, HD:HD + 1]).astype(BF)


def gather_kernel(o_ref, r_ref, ss, rs):
    sp = lax.axis_index("sp")
    z, x = sp // XN, lax.rem(sp, XN)
    bar = pltpu.get_barrier_semaphore()
    for d in (1, 2, 3):
        pl.semaphore_signal(bar, inc=1, device_id=sp_of(z + d, x), device_id_type=MESH)
    pl.semaphore_wait(bar, 3)
    cs = []
    for d in (1, 3, 2):
        c = pltpu.make_async_remote_copy(o_ref.at[lax.rem(z + d, ZN)], r_ref.at[z], ss.at[d - 1], rs.at[d - 1],
                                         device_id=sp_of(z + d, x), device_id_type=MESH)
        c.start()
        cs.append(c)
    r_ref[z] = o_ref[z]
    for c in cs:
        c.wait()


def project_kernel(slot_ref, t_ref, w_ref, r_ref, g_ref, u_ref, out_ref, u2, sq, n3):
    i = pl.program_id(0)
    nb = w_ref.shape[1]
    y = r_ref[...].astype(F32)
    acc = jnp.dot(t_ref[0], w_ref[0:512, :], preferred_element_type=F32)
    for k in range(1, 4):
        acc = acc + jnp.dot(t_ref[k], w_ref[k * 512:(k + 1) * 512, :], preferred_element_type=F32)
    u = (y + acc).astype(BF)
    u_ref[...] = u
    wide = u.astype(F32)
    u2[i] = wide
    part = jnp.sum(wide * wide, axis=-1, keepdims=True)

    @pl.when(i == 0)
    def _():
        sq[...] = part

    @pl.when(i > 0)
    def _():
        sq[...] += part

    @pl.when(i == pl.num_programs(0) - 1)
    def _():
        inv = lax.rsqrt(sq[...] / 2048.0 + EPSILON)
        per = nb // HD
        for j in range(16):
            piece = u2[j // per, :, (j % per) * HD:(j % per + 1) * HD]
            n3[:, j, :] = (piece * inv * g_ref[:, j * HD:(j + 1) * HD]).astype(BF).astype(F32)

        def slot(s, _):
            out_ref[s] = n3[slot_ref[0, s]].astype(BF)
            return 0

        lax.fori_loop(0, N_DEV * CAP, slot, 0, unroll=8)


def swap_kernel(a_ref, b_ref, ss, rs):
    me = lax.axis_index("sp") * 8 + lax.axis_index("dp")
    bar = pltpu.get_barrier_semaphore()

    def dev(p):
        return {"sp": p // 8, "dp": lax.rem(p, 8)}

    def sig(i, _):
        pl.semaphore_signal(bar, inc=1, device_id=dev(lax.rem(me + i, N_DEV)), device_id_type=MESH)
        return 0

    lax.fori_loop(1, N_DEV, sig, 0)
    pl.semaphore_wait(bar, N_DEV - 1)

    def send(i, _):
        p = lax.rem(me + i * 37, N_DEV)
        pltpu.make_async_remote_copy(a_ref.at[p], b_ref.at[me], ss, rs, device_id=dev(p), device_id_type=MESH).start()
        return 0

    lax.fori_loop(1, N_DEV, send, 0)
    b_ref[me] = a_ref[me]
    rest = pl.ds(0, N_DEV - 1)
    pltpu.make_async_remote_copy(a_ref.at[rest], b_ref.at[rest], ss, rs, device_id=dev(me), device_id_type=MESH).wait()


def expert_kernel(x_ref, wg_ref, wu_ref, wd_ref, y_ref, w3, xs, act):
    i = pl.program_id(0)
    n = N_DEV * CAP

    @pl.when(i == 0)
    def _():
        def widen(t, _):
            rows = pl.ds(t * 8, 8)
            w3[rows] = x_ref[rows].astype(F32)
            return 0

        lax.fori_loop(0, n // 8, widen, 0, unroll=2)
        for j in range(16):
            xs[:, j * HD:(j + 1) * HD] = w3[:, j, :].astype(BF)

    @pl.when(i < 4)
    def _():
        x = xs[...]
        g = jnp.minimum(jnp.dot(x, wg_ref[...], preferred_element_type=F32), LIMIT)
        l = jnp.clip(jnp.dot(x, wu_ref[...], preferred_element_type=F32), -LIMIT, LIMIT)
        act[i] = (g * jax.nn.sigmoid(SLOPE * g) * (l + 1.0)).astype(BF)

    @pl.when(i >= 4)
    def _():
        y = jnp.dot(act[0], wd_ref[0:256, :], preferred_element_type=F32)
        for k in range(1, 4):
            y = y + jnp.dot(act[k], wd_ref[k * 256:(k + 1) * 256, :], preferred_element_type=F32)
        y = y.astype(BF).astype(F32)
        for jj in range(4):
            w3[:, (i - 4) * 4 + jj, :] = y[:, jj * HD:(jj + 1) * HD]

    @pl.when(i == 7)
    def _():
        def narrow(t, _):
            rows = pl.ds(t * 8, 8)
            y_ref[rows] = w3[rows].astype(BF)
            return 0

        lax.fori_loop(0, n // 8, narrow, 0, unroll=2)


def combine_kernel(tgt_ref, wt_ref, y_ref, u_ref, o_ref, c3):
    def token(t, _):
        a = y_ref[tgt_ref[0, 2 * t]].astype(F32) * wt_ref[0, 2 * t]
        b = y_ref[tgt_ref[0, 2 * t + 1]].astype(F32) * wt_ref[0, 2 * t + 1]
        c3[t] = a + b
        return 0

    lax.fori_loop(0, TOK, token, 0, unroll=8)
    for j in range(16):
        cols = slice(j * HD, (j + 1) * HD)
        o_ref[:, cols] = (u_ref[:, cols].astype(F32) + c3[:, j, :]).astype(BF)


def full(shape):
    return pl.BlockSpec(shape, lambda *i: (0,) * len(shape))


def per_device(resid, query, keys, values, q_gain, k_gain, out_weight, norm_gain, route_ids, route_weight,
               expert_gate, expert_up, expert_down):
    sds = jax.ShapeDtypeStruct
    sem = pltpu.SemaphoreType.DMA
    weight = lax.all_gather(out_weight, "dp", axis=0, tiled=True)
    places = lax.axis_index("sp") * TOK + jnp.arange(TOK, dtype=jnp.int32)
    cosine, sine = turn_tables(places)
    ids = route_ids[0].reshape(1, 2 * TOK)
    qs, kvs, target, slots = pl.pallas_call(
        prep_kernel,
        out_shape=(sds((4, TOK, 512), BF), sds((4, 2, TOK, HD), BF), sds((1, 2 * TOK), jnp.int32),
                   sds((1, N_DEV * CAP), jnp.int32)),
        compiler_params=params(), name="prep",
    )(query[0], keys[0], values[0], q_gain[None], k_gain[None], cosine, sine, ids, ids.reshape(2 * TOK, 1))
    qr, kvr = pl.pallas_call(
        spread_kernel,
        out_shape=(sds((4, TOK, 512), BF), sds((4, 4, 2, TOK, HD), BF)),
        in_specs=[VM, VM], out_specs=(VM, VM),
        scratch_shapes=[sem((3,)), sem((3,)), sem((3,)), sem((3,)), sem((2, 4)), sem((2, 4)), sem((4,)), sem((4,))],
        compiler_params=params(cid=0), name="spread",
    )(qs, kvs)
    heads = pl.pallas_call(
        attend_kernel,
        grid=(16,),
        out_shape=sds((4, TOK, 512), BF),
        in_specs=[pl.BlockSpec((1, TOK, HD), lambda i: (i // 4, 0, i % 4)), full((4, 4, 2, TOK, HD))],
        out_specs=pl.BlockSpec((1, TOK, HD), lambda i: (i // 4, 0, i % 4)),
        scratch_shapes=[pltpu.VMEM((4096, 256), BF)],
        compiler_params=params(), name="attend",
        cost_estimate=pl.CostEstimate(flops=17_000_000_000, bytes_accessed=4_000_000, transcendentals=16_000_000),
    )(qr, kvr)
    tok = pl.pallas_call(
        gather_kernel,
        out_shape=sds((4, TOK, 512), BF),
        in_specs=[VM], out_specs=VM,
        scratch_shapes=[sem((3,)), sem((3,))],
        compiler_params=params(cid=1), name="heads_back",
    )(heads)
    nb = 512
    updated, rows = pl.pallas_call(
        project_kernel,
        grid=(2048 // nb,),
        out_shape=(sds((TOK, 2048), BF), sds((N_DEV * CAP, 16, HD), BF)),
        in_specs=[SM, full((4, TOK, 512)), pl.BlockSpec((2048, nb), lambda i: (0, i)),
                  pl.BlockSpec((TOK, nb), lambda i: (0, i)), full((1, 2048))],
        out_specs=(pl.BlockSpec((TOK, nb), lambda i: (0, i)), full((N_DEV * CAP, 16, HD))),
        scratch_shapes=[pltpu.VMEM((2048 // nb, TOK, nb), F32), pltpu.VMEM((TOK, 1), F32),
                        pltpu.VMEM((TOK, 16, HD), F32)],
        compiler_params=params(), name="project",
    )(slots, tok, weight, resid[0], norm_gain[None])

    def swap(a, cid, name):
        return pl.pallas_call(
            swap_kernel,
            out_shape=sds((N_DEV, CAP, 16, HD), BF),
            in_specs=[VM], out_specs=VM,
            scratch_shapes=[sem, sem],
            compiler_params=params(cid=cid), name=name,
        )(a.reshape(N_DEV, CAP, 16, HD)).reshape(N_DEV * CAP, 16, HD)

    came = swap(rows, 2, "dispatch")
    n = N_DEV * CAP
    answered = pl.pallas_call(
        expert_kernel,
        grid=(8,),
        out_shape=sds((n, 16, HD), BF),
        in_specs=[full((n, 16, HD)), pl.BlockSpec((2048, 256), lambda i: (0, jnp.minimum(i, 3))),
                  pl.BlockSpec((2048, 256), lambda i: (0, jnp.minimum(i, 3))),
                  pl.BlockSpec((1024, 512), lambda i: (0, jnp.maximum(i - 4, 0)))],
        out_specs=full((n, 16, HD)),
        scratch_shapes=[pltpu.VMEM((n, 16, HD), F32), pltpu.VMEM((n, 2048), BF), pltpu.VMEM((4, n, 256), BF)],
        compiler_params=params(), name="expert",
    )(came, expert_gate[0], expert_up[0], expert_down[0])
    returned = swap(answered, 3, "answers_back")
    out = pl.pallas_call(
        combine_kernel,
        out_shape=sds((TOK, 2048), BF),
        in_specs=[SM, SM, VM, VM], out_specs=VM,
        scratch_shapes=[pltpu.VMEM((TOK, 16, HD), F32)],
        compiler_params=params(), name="combine",
    )(target, route_weight[0].reshape(1, 2 * TOK), returned, updated)
    return out[None]


def solution(mesh):
    placed = (
        P("dp", "sp", None),
        P("dp", "sp", None),
        P("dp", "sp", None),
        P("dp", "sp", None),
        P(),
        P(),
        P("dp", None),
        P(),
        P("dp", "sp", None),
        P("dp", "sp", None),
        P(("sp", "dp"), None, None),
        P(("sp", "dp"), None, None),
        P(("sp", "dp"), None, None),
    )
    return jax.shard_map(
        per_device, mesh=mesh, in_specs=placed, out_specs=P("dp", "sp", None), check_vma=False
    )
```

time: 346 us -> 231 us (0.67)
  Pallas kernels: 0 us -> 204 us
  waiting for transfers between devices: 97.9 us -> 0.73 us
  blocking collectives: 60.4 us -> 0 us
  matrix products: 59.4 us -> 0 us
  local copies, waits for them, and re-layouts: 44.9 us -> 9.05 us
  starting transfers between devices: 35.2 us -> 0.01 us
  other arithmetic: 31.1 us -> 0.58 us
    pallas_call x0 -> x9, Pallas kernels: none -> 204 us  [the longest x2 92.3 us: swap(): pl.pallas_call(swap_kernel, out_shape=sds((N_DEV, CAP, 16, HD), BF), in_s...]
    all_to_all x5 -> x0, waiting for transfers between devices: 97.2 us -> none  [the longest x1 51.5 us: per_device(): lax.all_to_all(answered, ('sp', 'dp'), split_axis=0, concat_axis=0, tiled...]
    all_to_all x1 -> x0, blocking collectives: 60.4 us -> none  [per_device(): lax.all_to_all(outgoing, ('sp', 'dp'), split_axis=0, concat_axis=0, tiled...]
    dot_general x20 -> x0, matrix products: 59.4 us -> none  [the longest x8 29.6 us: one_block(): jnp.einsum('kgqs,skd->qkgd', attn_weights, head_value, preferred_element_...]
    all_to_all x5 -> x0, starting transfers between devices: 35.2 us -> none  [the longest x1 8.26 us: per_device(): lax.all_to_all(key_turned, 'sp', split_axis=1, concat_axis=0, tiled=True)]
    reduce_sum x12 -> x0, other arithmetic: 21.8 us -> none  [the longest x8 12 us: one_block(): jnp.sum(lifted, axis=-1, keepdims=True)]
    reshape x5 -> x0, local copies, waits for them, and re-layouts: 19.3 us -> none  [the longest x1 6.25 us: per_device(): outgoing = padded[slot_table].reshape(experts_total, capacity, model_width)]
    gather x2 -> x0, local copies, waits for them, and re-layouts: 7.6 us -> none  [the longest x1 4.27 us: per_device(): outgoing = padded[slot_table].reshape(experts_total, capacity, model_width)]
  transfers between devices with their start and end apart: 6 -> 1, of which waited for: 5 -> 0; matrix products, arithmetic and copies ran while one was open for 19% -> 1% of each run, Pallas kernels for 0% -> 32%
where the time goes in v1:
time: 231 us; the launch traced here: 228 us
  Pallas kernels  204 us (88%)
  between operations  13.6 us (6%)
  local copies, waits for them, and re-layouts  9.05 us (4%)
    pallas_call x2, Pallas kernels, swap(): pl.pallas_call(swap_kernel, out_shape=sds((N_DEV, CAP, 16, HD), BF), in_s...  92.3 us
    pallas_call x1, Pallas kernels, per_device(): pl.pallas_call(attend_kernel, grid=(16,), out_shape=sds((4, TOK, 512), BF...  30.5 us
    pallas_call x1, Pallas kernels, per_device(): pl.pallas_call(spread_kernel, out_shape=(sds((4, TOK, 512), BF), sds((4,...  27.2 us
    pallas_call x1, Pallas kernels, per_device(): pl.pallas_call(expert_kernel, grid=(8,), out_shape=sds((n, 16, HD), BF),...  24.8 us
    pallas_call x1, Pallas kernels, per_device(): pl.pallas_call(gather_kernel, out_shape=sds((4, TOK, 512), BF), in_specs=...  10.8 us
    pallas_call x1, Pallas kernels, per_device(): pl.pallas_call(project_kernel, grid=(2048 // nb,), out_shape=(sds((TOK, 2...  10.8 us
    unnamed x22, local copies, waits for them, and re-layouts  8.67 us
  transfers between devices with their start and end apart: 1, of which 0 were waited for; matrix products, arithmetic and copies ran while one was open for 1% of the time, Pallas kernels for 32%

profile of v1, /device:TPU:6, one launch (start us, length us, event | category | flops | bytes accessed | tf_op | source)
XLA Modules:
  0.0 228.2 jit_solution(7860022699343830124)
XLA Ops:
  6.5 0.7 all-gather.2.cloned.1.call-update
  7.3 0.8 copy.17
  8.1 0.1 reshape_reshape_squeeze.4.idc_ref
  8.2 0.1 reshape_squeeze.6.idr_ref
  8.4 0.6 sine_multiply_fusion
  8.9 1.2 copy-done.2
  10.2 0.9 copy-done.4
  11.1 0.9 copy-done.5
  12.1 0.7 copy-done.7
  12.7 0.7 copy-done.8
  13.4 4.0 %prep.1 = (bf16[4,256,512]{2,1,0:T(8,128)(2,1)S(1)}, bf16[4,2,256,128]{3,2,1,0:T(8,128)(2,1)S(1)}, s32[1,512]{1,0:T(1,128)S(1)}, s32[1,768]{1,0:T(1,128)S(1)}) custom-call(bf16[256,2048]{1,0:T(8,128)(2,1)S(1)} %bitcast.18, bf16[256,512]{1,0:T(8,128)(2,1)S(1)} %bitcast.20, bf16[256,512]{1,0:T(8,128)(2,1)S(1)} %bitcast.21, f32[1,128]{1,0:T(1,128)S(1)} %bitcast.23, ...), custom_call_target="tpu_custom_call" | custom-call | tf_op jit(solution)/shard_map/prep/pallas_call | solution.py:306
  17.4 27.2 %spread.1 = (bf16[4,256,512]{2,1,0:T(8,128)(2,1)S(1)}, bf16[4,4,2,256,128]{4,3,2,1,0:T(8,128)(2,1)S(1)}) custom-call(bf16[4,256,512]{2,1,0:T(8,128)(2,1)S(1)} %get-tuple-element.15.qs_ref, bf16[4,2,256,128]{3,2,1,0:T(8,128)(2,1)S(1)} %get-tuple-element.16.kvs_ref), custom_call_target="tpu_custom_call" | custom-call | tf_op jit(solution)/shard_map/spread/pallas_call | solution.py:312
  44.6 30.5 %attend.1.o_ref = bf16[4,256,512]{2,1,0:T(8,128)(2,1)S(1)} custom-call(bf16[4,256,512]{2,1,0:T(8,128)(2,1)S(1)} %get-tuple-element.17.q_ref, bf16[4,4,2,256,128]{4,3,2,1,0:T(8,128)(2,1)S(1)} %get-tuple-element.18.kv_ref), custom_call_target="tpu_custom_call" | custom-call | flops 16999999488 | bytes 4000000 | tf_op jit(solution)/shard_map/attend/pallas_call | solution.py:319
  75.1 10.8 %heads_back.1.t_ref = bf16[4,256,512]{2,1,0:T(8,128)(2,1)S(1)} custom-call(bf16[4,256,512]{2,1,0:T(8,128)(2,1)S(1)} %attend.1.o_ref), custom_call_target="tpu_custom_call" | custom-call | tf_op jit(solution)/shard_map/heads_back/pallas_call | solution.py:329
  86.0 0.1 copy.20
  86.1 0.1 reshape_squeeze.7.wt_ref
  86.3 0.0 all-gather.2.cloned.1.call-done.w_ref
  86.3 10.8 %project.1 = (bf16[256,2048]{1,0:T(8,128)(2,1)S(1)}, bf16[768,16,128]{2,1,0:T(8,128)(2,1)}) custom-call(s32[1,768]{1,0:T(1,128)S(1)} %get-tuple-element.14.slot_ref, bf16[4,256,512]{2,1,0:T(8,128)(2,1)S(1)} %heads_back.1.t_ref, bf16[2048,2048]{1,0:T(8,128)(2,1)} %all-gather.2.cloned.1.call-done.w_ref, bf16[256,2048]{1,0:T(8,128)(2,1)S(1)} %bitcast.19, ...), custom_call_target="tpu_custom_call" | custom-call | tf_op jit(solution)/shard_map/project/pallas_call | solution.py:337
  97.1 46.2 %dispatch.1 = bf16[128,6,16,128]{3,2,1,0:T(8,128)(2,1)S(1)} custom-call(bf16[128,6,16,128]{3,2,1,0:T(8,128)(2,1)} %bitcast.28), custom_call_target="tpu_custom_call" | custom-call | tf_op jit(solution)/shard_map/dispatch/pallas_call | solution.py:350
  143.3 1.6 copy-done
  144.9 24.8 %expert.1 = bf16[768,16,128]{2,1,0:T(8,128)(2,1)S(1)} custom-call(bf16[768,16,128]{2,1,0:T(8,128)(2,1)} %bitcast.15, bf16[2048,1024]{1,0:T(8,128)(2,1)} %bitcast.25, bf16[2048,1024]{1,0:T(8,128)(2,1)} %bitcast.26, bf16[1024,2048]{1,0:T(8,128)(2,1)} %bitcast.27), custom_call_target="tpu_custom_call" | custom-call | tf_op jit(solution)/shard_map/expert/pallas_call | solution.py:360
  169.8 1.6 copy-done.1
  171.4 46.1 %answers_back.1 = bf16[128,6,16,128]{3,2,1,0:T(8,128)(2,1)S(1)} custom-call(bf16[128,6,16,128]{3,2,1,0:T(8,128)(2,1)} %bitcast.16), custom_call_target="tpu_custom_call" | custom-call | tf_op jit(solution)/shard_map/answers_back/pallas_call | solution.py:350
  217.5 3.8 %combine.1 = bf16[256,2048]{1,0:T(8,128)(2,1)} custom-call(s32[1,512]{1,0:T(1,128)S(1)} %get-tuple-element.13.tgt_ref, f32[1,512]{1,0:T(1,128)S(1)} %reshape_squeeze.7.wt_ref, bf16[768,16,128]{2,1,0:T(8,128)(2,1)S(1)} %bitcast.17, bf16[256,2048]{1,0:T(8,128)(2,1)S(1)} %get-tuple-element.20.u_ref), custom_call_target="tpu_custom_call" | custom-call | tf_op jit(solution)/shard_map/combine/pallas_call | solution.py:372
  (17 shorter events, 0.1 us)
Async XLA Ops:
  6.5 79.8 %all-gather.2.cloned.1.call-start = ((), (), s32[]{:S(2)}) async-start(), calls=%async_computation | async-start | bytes 9437184 | tf_op jit(solution)/shard_map/all_gather | solution.py:302
  8.9 1.2 copy-start.2
  10.2 0.9 copy-start.4
  11.1 0.9 copy-start.5
  12.1 0.7 copy-start.7
  12.7 0.7 copy-start.8
  44.6 41.4 %copy-start.9 = (f32[1,256,2]{1,2,0:T(2,128)S(1)}, f32[1,256,2]{1,2,0:T(2,128)}, u32[]{:S(2)}) copy-start(f32[1,256,2]{1,2,0:T(2,128)} %param.22) | copy-start | bytes 6148
  44.6 41.8 %copy-start.3 = (bf16[1,256,2048]{2,1,0:T(8,128)(2,1)S(1)}, bf16[1,256,2048]{2,1,0:T(8,128)(2,1)}, u32[]{:S(2)}) copy-start(bf16[1,256,2048]{2,1,0:T(8,128)(2,1)} %param.13) | copy-start | bytes 3145732
  44.6 41.7 %copy-start.6 = (f32[2048]{0:T(1024)S(1)}, f32[2048]{0:T(1024)}, u32[]{:S(2)}) copy-start(f32[2048]{0:T(1024)} %param.20) | copy-start | bytes 24580
  143.3 1.6 copy-start
  169.8 1.6 copy-start.1
Sparse Core Ops, SparseCore 0:
  9.0 51.9 all-gather.1

commit v2 on v1

--- a/solution.py
+++ b/solution.py
@@ -176,7 +176,7 @@
         c.wait()
 
 
-def project_kernel(slot_ref, t_ref, w_ref, r_ref, g_ref, u_ref, out_ref, u2, sq, n3):
+def project_kernel(t_ref, w_ref, r_ref, g_ref, u_ref, out_ref, u2, sq, n3):
     i = pl.program_id(0)
     nb = w_ref.shape[1]
     y = r_ref[...].astype(F32)
@@ -205,87 +205,146 @@
             piece = u2[j // per, :, (j % per) * HD:(j % per + 1) * HD]
             n3[:, j, :] = (piece * inv * g_ref[:, j * HD:(j + 1) * HD]).astype(BF).astype(F32)
 
-        def slot(s, _):
-            out_ref[s] = n3[slot_ref[0, s]].astype(BF)
+        def narrow(t, _):
+            rows = pl.ds(t * 8, 8)
+            out_ref[rows] = n3[rows].astype(BF)
             return 0
 
-        lax.fori_loop(0, N_DEV * CAP, slot, 0, unroll=8)
-
-
-def swap_kernel(a_ref, b_ref, ss, rs):
+        lax.fori_loop(0, TOK // 8, narrow, 0)
+
+
+GROUPS = 4
+PER = N_DEV // GROUPS
+STEP = 37
+
+
+def moe_kernel(slot_ref, tgt_ref, wt_ref, n_ref, u_ref, wg_hbm, wu_hbm, wd_hbm, o_ref,
+               wg, wu, wd, rows, came, y, ret, w3, xs, act, c3, wsem, ss, rs, ys, yr):
     me = lax.axis_index("sp") * 8 + lax.axis_index("dp")
     bar = pltpu.get_barrier_semaphore()
+    n = PER * CAP
 
     def dev(p):
         return {"sp": p // 8, "dp": lax.rem(p, 8)}
+
+    def ahead(i):
+        return lax.rem(me + i * STEP, N_DEV)
+
+    def behind(i):
+        return lax.rem(me + i * (N_DEV - STEP), N_DEV)
 
     def sig(i, _):
         pl.semaphore_signal(bar, inc=1, device_id=dev(lax.rem(me + i, N_DEV)), device_id_type=MESH)
         return 0
 
     lax.fori_loop(1, N_DEV, sig, 0)
+    loads = []
+    for k in range(4):
+        for src, dst in ((wg_hbm.at[:, k * 256:(k + 1) * 256], wg.at[k]), (wu_hbm.at[:, k * 256:(k + 1) * 256], wu.at[k]),
+                         (wd_hbm.at[:, k * 512:(k + 1) * 512], wd.at[k])):
+            c = pltpu.make_async_copy(src, dst, wsem.at[len(loads)])
+            c.start()
+            loads.append(c)
+
+    def pick(i, _):
+        p = ahead(i)
+        for r in range(CAP):
+            rows[i, r] = n_ref[slot_ref[0, p * CAP + r]]
+        return 0
+
+    def send(i, _):
+        p = ahead(i)
+        pltpu.make_async_remote_copy(rows.at[i], came.at[i], ss, rs.at[i // PER], device_id=dev(p), device_id_type=MESH).start()
+        return 0
+
+    lax.fori_loop(0, PER, pick, 0)
+    came[0] = rows[0]
     pl.semaphore_wait(bar, N_DEV - 1)
-
-    def send(i, _):
-        p = lax.rem(me + i * 37, N_DEV)
-        pltpu.make_async_remote_copy(a_ref.at[p], b_ref.at[me], ss, rs, device_id=dev(p), device_id_type=MESH).start()
-        return 0
-
-    lax.fori_loop(1, N_DEV, send, 0)
-    b_ref[me] = a_ref[me]
-    rest = pl.ds(0, N_DEV - 1)
-    pltpu.make_async_remote_copy(a_ref.at[rest], b_ref.at[rest], ss, rs, device_id=dev(me), device_id_type=MESH).wait()
-
-
-def expert_kernel(x_ref, wg_ref, wu_ref, wd_ref, y_ref, w3, xs, act):
-    i = pl.program_id(0)
-    n = N_DEV * CAP
-
-    @pl.when(i == 0)
-    def _():
+    lax.fori_loop(1, PER, send, 0)
+    for g in range(1, GROUPS):
+        lax.fori_loop(g * PER, (g + 1) * PER, pick, 0)
+        lax.fori_loop(g * PER, (g + 1) * PER, send, 0)
+    for c in loads:
+        c.wait()
+
+    def group(g, _):
+        base = g * PER
+
+        def arrived(first, count, sem):
+            part = pl.ds(first, count)
+            pltpu.make_async_remote_copy(rows.at[part], came.at[part], ss, sem, device_id=dev(me), device_id_type=MESH).wait_recv()
+
+        @pl.when(g == 0)
+        def _():
+            arrived(1, PER - 1, rs.at[0])
+
+        @pl.when(g > 0)
+        def _():
+            arrived(base, PER, rs.at[g])
+
         def widen(t, _):
-            rows = pl.ds(t * 8, 8)
-            w3[rows] = x_ref[rows].astype(F32)
+            for r in range(CAP):
+                w3[t * CAP + r] = came[base + t, r].astype(F32)
             return 0
 
-        lax.fori_loop(0, n // 8, widen, 0, unroll=2)
+        lax.fori_loop(0, PER, widen, 0)
         for j in range(16):
             xs[:, j * HD:(j + 1) * HD] = w3[:, j, :].astype(BF)
 
-    @pl.when(i < 4)
-    def _():
-        x = xs[...]
-        g = jnp.minimum(jnp.dot(x, wg_ref[...], preferred_element_type=F32), LIMIT)
-        l = jnp.clip(jnp.dot(x, wu_ref[...], preferred_element_type=F32), -LIMIT, LIMIT)
-        act[i] = (g * jax.nn.sigmoid(SLOPE * g) * (l + 1.0)).astype(BF)
-
-    @pl.when(i >= 4)
-    def _():
-        y = jnp.dot(act[0], wd_ref[0:256, :], preferred_element_type=F32)
-        for k in range(1, 4):
-            y = y + jnp.dot(act[k], wd_ref[k * 256:(k + 1) * 256, :], preferred_element_type=F32)
-        y = y.astype(BF).astype(F32)
-        for jj in range(4):
-            w3[:, (i - 4) * 4 + jj, :] = y[:, jj * HD:(jj + 1) * HD]
-
-    @pl.when(i == 7)
-    def _():
+        def up(k, _):
+            x = xs[...]
+            a = jnp.minimum(jnp.dot(x, wg[k], preferred_element_type=F32), LIMIT)
+            b = jnp.clip(jnp.dot(x, wu[k], preferred_element_type=F32), -LIMIT, LIMIT)
+            act[k] = (a * jax.nn.sigmoid(SLOPE * a) * (b + 1.0)).astype(BF)
+            return 0
+
+        lax.fori_loop(0, 4, up, 0)
+
+        for k in range(4):
+            d = jnp.dot(act[0], wd[k, 0:256, :], preferred_element_type=F32)
+            for m in range(1, 4):
+                d = d + jnp.dot(act[m], wd[k, m * 256:(m + 1) * 256, :], preferred_element_type=F32)
+            for j in range(4):
+                w3[:, k * 4 + j, :] = d[:, j * HD:(j + 1) * HD]
+
         def narrow(t, _):
-            rows = pl.ds(t * 8, 8)
-            y_ref[rows] = w3[rows].astype(BF)
+            for r in range(CAP):
+                y[base + t, r] = w3[t * CAP + r].astype(BF)
             return 0
 
-        lax.fori_loop(0, n // 8, narrow, 0, unroll=2)
-
-
-def combine_kernel(tgt_ref, wt_ref, y_ref, u_ref, o_ref, c3):
+        lax.fori_loop(0, PER, narrow, 0)
+
+        def answer(t, _):
+            i = base + t
+            pltpu.make_async_remote_copy(y.at[i], ret.at[me], ys, yr, device_id=dev(behind(i)), device_id_type=MESH).start()
+            return 0
+
+        @pl.when(g == 0)
+        def _():
+            ret[me] = y[0]
+            lax.fori_loop(1, PER, answer, 0)
+
+        @pl.when(g > 0)
+        def _():
+            lax.fori_loop(0, PER, answer, 0)
+
+        return 0
+
+    lax.fori_loop(0, GROUPS, group, 0)
+    rest = pl.ds(0, N_DEV - 1)
+    pltpu.make_async_remote_copy(y.at[rest], ret.at[rest], ys, yr, device_id=dev(me), device_id_type=MESH).wait()
+    pltpu.make_async_remote_copy(rows.at[rest], came.at[rest], ss, rs.at[0], device_id=dev(me), device_id_type=MESH).wait_send()
+
     def token(t, _):
-        a = y_ref[tgt_ref[0, 2 * t]].astype(F32) * wt_ref[0, 2 * t]
-        b = y_ref[tgt_ref[0, 2 * t + 1]].astype(F32) * wt_ref[0, 2 * t + 1]
-        c3[t] = a + b
+        for h in range(4):
+            q = t * 4 + h
+            i0, i1 = tgt_ref[0, 2 * q], tgt_ref[0, 2 * q + 1]
+            a = ret[i0 // CAP, lax.rem(i0, CAP)].astype(F32) * wt_ref[0, 2 * q]
+            b = ret[i1 // CAP, lax.rem(i1, CAP)].astype(F32) * wt_ref[0, 2 * q + 1]
+            c3[q] = a + b
         return 0
 
-    lax.fori_loop(0, TOK, token, 0, unroll=8)
+    lax.fori_loop(0, TOK // 4, token, 0)
     for j in range(16):
         cols = slice(j * HD, (j + 1) * HD)
         o_ref[:, cols] = (u_ref[:, cols].astype(F32) + c3[:, j, :]).astype(BF)
@@ -337,45 +396,27 @@
     updated, rows = pl.pallas_call(
         project_kernel,
         grid=(2048 // nb,),
-        out_shape=(sds((TOK, 2048), BF), sds((N_DEV * CAP, 16, HD), BF)),
-        in_specs=[SM, full((4, TOK, 512)), pl.BlockSpec((2048, nb), lambda i: (0, i)),
+        out_shape=(sds((TOK, 2048), BF), sds((TOK, 16, HD), BF)),
+        in_specs=[full((4, TOK, 512)), pl.BlockSpec((2048, nb), lambda i: (0, i)),
                   pl.BlockSpec((TOK, nb), lambda i: (0, i)), full((1, 2048))],
-        out_specs=(pl.BlockSpec((TOK, nb), lambda i: (0, i)), full((N_DEV * CAP, 16, HD))),
+        out_specs=(pl.BlockSpec((TOK, nb), lambda i: (0, i)), full((TOK, 16, HD))),
         scratch_shapes=[pltpu.VMEM((2048 // nb, TOK, nb), F32), pltpu.VMEM((TOK, 1), F32),
                         pltpu.VMEM((TOK, 16, HD), F32)],
         compiler_params=params(), name="project",
-    )(slots, tok, weight, resid[0], norm_gain[None])
-
-    def swap(a, cid, name):
-        return pl.pallas_call(
-            swap_kernel,
-            out_shape=sds((N_DEV, CAP, 16, HD), BF),
-            in_specs=[VM], out_specs=VM,
-            scratch_shapes=[sem, sem],
-            compiler_params=params(cid=cid), name=name,
-        )(a.reshape(N_DEV, CAP, 16, HD)).reshape(N_DEV * CAP, 16, HD)
-
-    came = swap(rows, 2, "dispatch")
-    n = N_DEV * CAP
-    answered = pl.pallas_call(
-        expert_kernel,
-        grid=(8,),
-        out_shape=sds((n, 16, HD), BF),
-        in_specs=[full((n, 16, HD)), pl.BlockSpec((2048, 256), lambda i: (0, jnp.minimum(i, 3))),
-                  pl.BlockSpec((2048, 256), lambda i: (0, jnp.minimum(i, 3))),
-                  pl.BlockSpec((1024, 512), lambda i: (0, jnp.maximum(i - 4, 0)))],
-        out_specs=full((n, 16, HD)),
-        scratch_shapes=[pltpu.VMEM((n, 16, HD), F32), pltpu.VMEM((n, 2048), BF), pltpu.VMEM((4, n, 256), BF)],
-        compiler_params=params(), name="expert",
-    )(came, expert_gate[0], expert_up[0], expert_down[0])
-    returned = swap(answered, 3, "answers_back")
+    )(tok, weight, resid[0], norm_gain[None])
+
+    tiles = pltpu.VMEM((N_DEV, CAP, 16, HD), BF)
+    n = PER * CAP
     out = pl.pallas_call(
-        combine_kernel,
+        moe_kernel,
         out_shape=sds((TOK, 2048), BF),
-        in_specs=[SM, SM, VM, VM], out_specs=VM,
-        scratch_shapes=[pltpu.VMEM((TOK, 16, HD), F32)],
-        compiler_params=params(), name="combine",
-    )(target, route_weight[0].reshape(1, 2 * TOK), returned, updated)
+        in_specs=[SM, SM, SM, VM, VM] + [pl.BlockSpec(memory_space=pl.ANY)] * 3, out_specs=VM,
+        scratch_shapes=[pltpu.VMEM((4, 2048, 256), BF), pltpu.VMEM((4, 2048, 256), BF), pltpu.VMEM((4, 1024, 512), BF),
+                        tiles, tiles, tiles, tiles, pltpu.VMEM((n, 16, HD), F32), pltpu.VMEM((n, 2048), BF),
+                        pltpu.VMEM((4, n, 256), BF), pltpu.VMEM((TOK, 16, HD), F32),
+                        sem((12,)), sem, sem((GROUPS,)), sem, sem],
+        compiler_params=params(cid=2), name="moe",
+    )(slots, target, route_weight[0].reshape(1, 2 * TOK), rows, updated, expert_gate[0], expert_up[0], expert_down[0])
     return out[None]
 
 

time: 231 us -> 190 us (0.82)
  Pallas kernels: 204 us -> 166 us
    pallas_call x4 -> x1, Pallas kernels: 121 us -> 85.4 us  [per_device(): pl.pallas_call(moe_kernel, out_shape=sds((TOK, 2048), BF), in_specs=[SM,...]
    pallas_call x1, Pallas kernels: 10.8 us -> 7.96 us  [per_device(): pl.pallas_call(project_kernel, grid=(2048 // nb,), out_shape=(sds((TOK, 2...]
    unnamed x22 -> x19, local copies, waits for them, and re-layouts: 8.67 us -> 6.36 us
  transfers between devices with their start and end apart: 1 -> 1, of which waited for: 0 -> 0; matrix products, arithmetic and copies ran while one was open for 1% -> 1% of each run, Pallas kernels for 32% -> 39%
where the time goes in v2:
time: 190 us; the launch traced here: 188 us
  Pallas kernels  166 us (87%)
  between operations  13.6 us (7%)
  local copies, waits for them, and re-layouts  6.75 us (4%)
    pallas_call x1, Pallas kernels, per_device(): pl.pallas_call(moe_kernel, out_shape=sds((TOK, 2048), BF), in_specs=[SM,...  85.4 us
    pallas_call x1, Pallas kernels, per_device(): pl.pallas_call(attend_kernel, grid=(16,), out_shape=sds((4, TOK, 512), BF...  30.7 us
    pallas_call x1, Pallas kernels, per_device(): pl.pallas_call(spread_kernel, out_shape=(sds((4, TOK, 512), BF), sds((4,...  27.2 us
    pallas_call x1, Pallas kernels, per_device(): pl.pallas_call(gather_kernel, out_shape=sds((4, TOK, 512), BF), in_specs=...  10.8 us
    pallas_call x1, Pallas kernels, per_device(): pl.pallas_call(project_kernel, grid=(2048 // nb,), out_shape=(sds((TOK, 2...  7.96 us
    unnamed x19, local copies, waits for them, and re-layouts  6.36 us
    pallas_call x1, Pallas kernels, per_device(): pl.pallas_call(prep_kernel, out_shape=(sds((4, TOK, 512), BF), sds((4, 2,...  4.01 us
  transfers between devices with their start and end apart: 1, of which 0 were waited for; matrix products, arithmetic and copies ran while one was open for 1% of the time, Pallas kernels for 39%

profile of v2, /device:TPU:6, one launch (start us, length us, event | category | flops | bytes accessed | tf_op | source)
XLA Modules:
  0.0 187.7 jit_solution(15541401116791732228)
XLA Ops:
  6.5 0.7 all-gather.2.cloned.1.call-update
  7.3 0.8 copy.17
  8.1 0.1 reshape_reshape_squeeze.4.idc_ref
  8.2 0.1 reshape_squeeze.6.idr_ref
  8.4 0.6 sine_multiply_fusion
  8.9 0.0 copy-start.1
  8.9 1.2 copy-done.1
  10.2 0.9 copy-done.2
  11.1 0.9 copy-done.3
  12.1 0.7 copy-done.5
  12.7 0.7 copy-done.6
  13.4 4.0 %prep.1 = (bf16[4,256,512]{2,1,0:T(8,128)(2,1)S(1)}, bf16[4,2,256,128]{3,2,1,0:T(8,128)(2,1)S(1)}, s32[1,512]{1,0:T(1,128)S(1)}, s32[1,768]{1,0:T(1,128)S(1)}) custom-call(bf16[256,2048]{1,0:T(8,128)(2,1)S(1)} %bitcast.13, bf16[256,512]{1,0:T(8,128)(2,1)S(1)} %bitcast.14, bf16[256,512]{1,0:T(8,128)(2,1)S(1)} %bitcast.15, f32[1,128]{1,0:T(1,128)S(1)} %bitcast.17, ...), custom_call_target="tpu_custom_call" | custom-call | tf_op jit(solution)/shard_map/prep/pallas_call | solution.py:365
  17.4 27.2 %spread.1 = (bf16[4,256,512]{2,1,0:T(8,128)(2,1)S(1)}, bf16[4,4,2,256,128]{4,3,2,1,0:T(8,128)(2,1)S(1)}) custom-call(bf16[4,256,512]{2,1,0:T(8,128)(2,1)S(1)} %get-tuple-element.15.qs_ref, bf16[4,2,256,128]{3,2,1,0:T(8,128)(2,1)S(1)} %get-tuple-element.16.kvs_ref), custom_call_target="tpu_custom_call" | custom-call | tf_op jit(solution)/shard_map/spread/pallas_call | solution.py:371
  44.6 0.0 copy-start.7
  44.6 0.0 copy-start
  44.6 0.0 copy-start.4
  44.6 30.7 %attend.1.o_ref = bf16[4,256,512]{2,1,0:T(8,128)(2,1)S(1)} custom-call(bf16[4,256,512]{2,1,0:T(8,128)(2,1)S(1)} %get-tuple-element.17.q_ref, bf16[4,4,2,256,128]{4,3,2,1,0:T(8,128)(2,1)S(1)} %get-tuple-element.18.kv_ref), custom_call_target="tpu_custom_call" | custom-call | flops 16999999488 | bytes 4000000 | tf_op jit(solution)/shard_map/attend/pallas_call | solution.py:378
  75.3 10.8 %heads_back.1.t_ref = bf16[4,256,512]{2,1,0:T(8,128)(2,1)S(1)} custom-call(bf16[4,256,512]{2,1,0:T(8,128)(2,1)S(1)} %attend.1.o_ref), custom_call_target="tpu_custom_call" | custom-call | tf_op jit(solution)/shard_map/heads_back/pallas_call | solution.py:388
  86.2 0.1 copy.20
  86.3 0.1 reshape_squeeze.7.wt_ref
  86.5 0.0 all-gather.2.cloned.1.call-done.w_ref
  86.5 8.0 %project.1 = (bf16[256,2048]{1,0:T(8,128)(2,1)S(1)}, bf16[256,16,128]{2,1,0:T(8,128)(2,1)S(1)}) custom-call(bf16[4,256,512]{2,1,0:T(8,128)(2,1)S(1)} %heads_back.1.t_ref, bf16[2048,2048]{1,0:T(8,128)(2,1)} %all-gather.2.cloned.1.call-done.w_ref, bf16[256,2048]{1,0:T(8,128)(2,1)S(1)} %bitcast.12, f32[1,2048]{1,0:T(1,128)S(1)} %bitcast.16), custom_call_target="tpu_custom_call" | custom-call | tf_op jit(solution)/shard_map/project/pallas_call | solution.py:396
  94.5 85.4 %moe.1 = bf16[256,2048]{1,0:T(8,128)(2,1)S(1)} custom-call(s32[1,768]{1,0:T(1,128)S(1)} %get-tuple-element.13.slot_ref, s32[1,512]{1,0:T(1,128)S(1)} %get-tuple-element.14.tgt_ref, f32[1,512]{1,0:T(1,128)S(1)} %reshape_squeeze.7.wt_ref, bf16[256,16,128]{2,1,0:T(8,128)(2,1)S(1)} %get-tuple-element.19.n_ref, bf16[256,2048]{1,0:T(8,128)(2,1)S(1)} %get-tuple-element.20.u_ref, ...), custom_call_target="tpu_custom_call" | custom-call | tf_op jit(solution)/shard_map/moe/pallas_call | solution.py:410
  179.9 1.0 copy.22
  (11 shorter events, 0.0 us)
Async XLA Ops:
  6.5 80.0 %all-gather.2.cloned.1.call-start = ((), (), s32[]{:S(2)}) async-start(), calls=%async_computation | async-start | bytes 9437184 | tf_op jit(solution)/shard_map/all_gather | solution.py:361
  8.9 1.2 copy-start.1
  10.2 0.9 copy-start.2
  11.1 0.9 copy-start.3
  12.1 0.7 copy-start.5
  12.7 0.7 copy-start.6
  44.6 41.6 %copy-start.7 = (f32[1,256,2]{1,2,0:T(2,128)S(1)}, f32[1,256,2]{1,2,0:T(2,128)}, u32[]{:S(2)}) copy-start(f32[1,256,2]{1,2,0:T(2,128)} %param.22) | copy-start | bytes 6148
  44.6 41.9 %copy-start = (bf16[1,256,2048]{2,1,0:T(8,128)(2,1)S(1)}, bf16[1,256,2048]{2,1,0:T(8,128)(2,1)}, u32[]{:S(2)}) copy-start(bf16[1,256,2048]{2,1,0:T(8,128)(2,1)} %param.13) | copy-start | bytes 3145732
  44.6 41.9 %copy-start.4 = (f32[2048]{0:T(1024)S(1)}, f32[2048]{0:T(1024)}, u32[]{:S(2)}) copy-start(f32[2048]{0:T(1024)} %param.20) | copy-start | bytes 24580
Sparse Core Ops, SparseCore 0:
  9.0 51.9 all-gather.1

commit v3 on v2

v3 whole, which is shorter than its diff:
```python
import functools
import jax
import jax.numpy as jnp
from jax import lax
from jax.experimental import pallas as pl
from jax.experimental.pallas import tpu as pltpu
from jax.sharding import PartitionSpec as P

GRID_W = 64
EPSILON = 1e-06
THETA = 10000.0
LIMIT = 7.0
SLOPE = 1.702
LOG2E = 1.4426950408889634
HD = 128
TOK = 256
ZN = 4
XN = 4
N_DEV = 128
CAP = 6
BF = jnp.bfloat16
F32 = jnp.float32
MESH = pl.DeviceIdType.MESH
VM = pl.BlockSpec(memory_space=pltpu.VMEM)
SM = pl.BlockSpec(memory_space=pltpu.SMEM)
MB = 1 << 20


def params(limit=48 * MB, cid=None, **kw):
    if cid is not None:
        kw.update(collective_id=cid, has_side_effects=True)
    return pltpu.CompilerParams(vmem_limit_bytes=limit, **kw)


def turn_tables(places):
    lane = jnp.arange(HD, dtype=jnp.int32)
    inverse = THETA ** (-(lane % 32).astype(F32) / 32)
    place = jnp.where(lane[None, :] < 64, (places // GRID_W)[:, None], (places % GRID_W)[:, None])
    angles = place.astype(F32) * inverse[None, :]
    sign = jnp.where(lane % 64 < 32, -1.0, 1.0)
    return jnp.cos(angles), jnp.sin(angles) * sign[None, :]


def turn_head(x, gain, cosine, sine, first):
    x = x.astype(F32)
    x = x * lax.rsqrt(jnp.mean(x * x, axis=-1, keepdims=True) + EPSILON) * gain
    other = jnp.where(first, pltpu.roll(x, HD - 32, 1), pltpu.roll(x, 32, 1))
    return (x * cosine + other * sine).astype(BF)


def sp_of(z, x):
    return {"sp": lax.rem(z, ZN) * XN + lax.rem(x, XN)}


def dp_of(y, c):
    return lax.rem(y, 4) * 2 + lax.rem(c, 2)


def route_tables(ids_ref, tgt_ref, slot_ref):
    n = 2 * TOK
    row = ids_ref[...].astype(F32)
    ia = lax.broadcasted_iota(jnp.int32, (n, n), 0)
    ib = lax.broadcasted_iota(jnp.int32, (n, n), 1)
    col = jnp.sum(jnp.where(ia == ib, row, 0.0), axis=1, keepdims=True)
    same = col == row
    before = jnp.sum(jnp.where(same & (ia < ib), 1.0, 0.0), axis=0, keepdims=True)
    tgt_ref[...] = (row * CAP + before).astype(jnp.int32)
    before_c = jnp.sum(jnp.where(same & (ib < ia), 1.0, 0.0), axis=1, keepdims=True)
    target = (col * CAP + before_c).astype(jnp.int32)
    slots = lax.broadcasted_iota(jnp.int32, (n, N_DEV * CAP), 1)
    token = (lax.broadcasted_iota(jnp.int32, (n, N_DEV * CAP), 0) // 2).astype(F32)
    slot_ref[...] = jnp.sum(jnp.where(target == slots, token, 0.0), axis=0, keepdims=True).astype(jnp.int32)


def attend(q, kv_ref, ve_ref):
    scale = HD ** -0.5 * LOG2E
    q = jnp.concatenate([q[:, h * HD:(h + 1) * HD] for h in range(4)], axis=0)
    m = acc = None
    for c in range(8):
        k = kv_ref[c // 2, (c % 2) * 2:(c % 2) * 2 + 2, 0].reshape(512, HD)
        s = lax.dot_general(q, k, (((1,), (1,)), ((), ())), preferred_element_type=F32)
        top = jnp.max(s, axis=-1, keepdims=True) * scale
        m_new = top if m is None else jnp.maximum(m, top)
        p = jnp.exp2(s * scale - m_new).astype(BF)
        part = jnp.dot(p, ve_ref[c * 512:(c + 1) * 512, :], preferred_element_type=F32)
        acc = part if acc is None else acc * jnp.exp2(m - m_new) + part
        m = m_new
    return (acc[:, :HD] / acc[:, HD:HD + 1]).astype(BF)


def front_kernel(q_hbm, k_hbm, v_hbm, r_hbm, w_hbm, cos_hbm, sin_hbm, qg_ref, kg_ref, ng_ref, ids_ref,
                 u_ref, n_ref, tgt_ref, slot_ref,
                 qv, kx, vx, rv, wv, cosv, sinv, qs, kvs, qr, kvr, ve, heads, tok, n3,
                 ls, zks, zkr, zqs, zqr, xs, xr, fs, fr, hs, hr, w1s, w1r, w2s, w2r, wss, wsr):
    sp, dp = lax.axis_index("sp"), lax.axis_index("dp")
    z, x = sp // XN, lax.rem(sp, XN)
    yy, core = dp // 2, lax.rem(dp, 2)
    above, below, mate = dp_of(yy + 1, core), dp_of(yy + 3, core), dp_of(yy, core + 1)
    far_shard = dp_of(yy + 2, core)
    bar = pltpu.get_barrier_semaphore()
    for d in (1, 2, 3):
        pl.semaphore_signal(bar, inc=1, device_id=sp_of(z + d, x), device_id_type=MESH)
    for d in (1, 3):
        pl.semaphore_signal(bar, inc=1, device_id=sp_of(z, x + d), device_id_type=MESH)
    for p in (above, below, mate):
        pl.semaphore_signal(bar, inc=1, device_id={"dp": p}, device_id_type=MESH)
    loads = {}
    for i, (name, src, dst) in enumerate((("w", w_hbm, wv.at[dp]), ("k", k_hbm, kx), ("cos", cos_hbm, cosv), ("sin", sin_hbm, sinv),
                                          ("v", v_hbm, vx), ("q", q_hbm, qv), ("r", r_hbm, rv))):
        loads[name] = pltpu.make_async_copy(src, dst, ls.at[i])
        loads[name].start()
    pending = []

    def remote(src, dst, ssem, rsem, dev):
        return pltpu.make_async_remote_copy(src, dst, ssem, rsem, device_id=dev, device_id_type=MESH)

    def send(src, dst, ssem, rsem, dev):
        c = remote(src, dst, ssem, rsem, dev)
        c.start()
        pending.append(c)
        return c

    pl.semaphore_wait(bar, 8)
    loads["w"].wait()
    near_w = {}
    for half in (0, 1):
        for s, p in ((0, above), (1, below)):
            h = half if s == 0 else 1 - half
            near_w[s, h] = send(wv.at[dp, h], wv.at[dp, h], w1s.at[s, h], w1r.at[s, h], {"dp": p})
    mates = [send(wv.at[dp], wv.at[dp], wss.at[0], wsr.at[0], {"dp": mate})]

    first = lax.broadcasted_iota(jnp.int32, (TOK, HD), 1) % 64 < 32
    for name in ("k", "cos", "sin", "v"):
        loads[name].wait()
    cosine, sine = cosv[...], sinv[...]
    zk = {}
    for h in range(4):
        kvs[h, 0] = turn_head(kx[:, h * HD:(h + 1) * HD], kg_ref[...], cosine, sine, first)
        kvs[h, 1] = vx[:, h * HD:(h + 1) * HD]
    for d in (1, 3, 2):
        zk[d] = send(kvs.at[lax.rem(z + d, ZN)], kvr.at[x, z], zks.at[d - 1], zkr.at[d - 1], sp_of(z + d, x))
    kvr[x, z] = kvs[z]

    def gather(d):
        chunk = lax.rem(z + ZN - d, ZN)
        return [send(kvr.at[x, chunk], kvr.at[x, chunk], xs.at[s, d], xr.at[s, d], sp_of(z, x + (1, 3)[s])) for s in (0, 1)]

    loads["q"].wait()

    def turn_query(d):
        zz = lax.rem(z + d, ZN)
        for h in range(4):
            cols = pl.ds(pl.multiple_of(zz * 512 + h * HD, HD), HD)
            val = turn_head(qv[:, cols], qg_ref[...], cosine, sine, first)
            if d:
                qs[zz, :, h * HD:(h + 1) * HD] = val
            else:
                qr[zz, :, h * HD:(h + 1) * HD] = val
        return zz

    near = {0: gather(0)}
    for d in (3, 2, 1):
        zz = turn_query(d)
        send(qs.at[zz], qr.at[z], zqs.at[d - 1], zqr.at[d - 1], sp_of(z + d, x))
    far = []

    def forward(d):
        chunk = lax.rem(z + ZN - d, ZN)
        s = 0 if d in (0, 1) else 1
        near[d][s].wait_recv()
        came = lax.rem(x + (3, 1)[s], XN)
        far.append(send(kvr.at[came, chunk], kvr.at[came, chunk], fs.at[d], fr.at[d], sp_of(z, x + (1, 3)[s])))

    zk[1].wait_recv()
    near[1] = gather(1)
    turn_query(0)
    forward(0)
    zk[3].wait_recv()
    near[3] = gather(3)
    zk[2].wait_recv()
    near[2] = gather(2)
    route_tables(ids_ref, tgt_ref, slot_ref)
    forward(1)
    near_w[0, 0].wait_recv()
    far_w = [send(wv.at[below, 0], wv.at[below, 0], w2s.at[0], w2r.at[0], {"dp": above})]
    near_w[1, 1].wait_recv()
    far_w.append(send(wv.at[above, 1], wv.at[above, 1], w2s.at[1], w2r.at[1], {"dp": below}))
    forward(3)
    forward(2)
    for d in (0, 1, 2, 3):
        s = 0 if d in (0, 1) else 1
        near[d][1 - s].wait_recv()
    for c in far:
        c.wait_recv()
    lane = lax.broadcasted_iota(jnp.int32, (1024, HD), 1)
    for c in range(4):
        ve[c * 1024:(c + 1) * 1024, :HD] = kvr[c, :, 1].reshape(1024, HD)
        ve[c * 1024:(c + 1) * 1024, HD:] = jnp.where(lane == 0, 1.0, 0.0).astype(BF)

    def block(t, _):
        a = lax.rem(z + 1 + t, ZN)

        @pl.when(t < 3)
        def _():
            remote(qs.at[a], qr.at[a], zqs.at[2 - t], zqr.at[2 - t], sp_of(a, x)).wait_recv()

        o = attend(qr[a], kvr, ve)
        for h in range(4):
            heads[a, :, h * HD:(h + 1) * HD] = o[h * TOK:(h + 1) * TOK]

        @pl.when(t < 3)
        def _():
            remote(heads.at[a], tok.at[z], hs.at[t], hr.at[t], sp_of(a, x)).start()

        @pl.when(t == 0)
        def _():
            near_w[0, 1].wait_recv()
            remote(wv.at[below], wv.at[below], wss.at[1], wsr.at[1], {"dp": mate}).start()
            near_w[1, 0].wait_recv()
            remote(wv.at[above], wv.at[above], wss.at[2], wsr.at[2], {"dp": mate}).start()

        @pl.when(t == 2)
        def _():
            for c in far_w:
                c.wait_recv()
            remote(wv.at[far_shard], wv.at[far_shard], wss.at[3], wsr.at[3], {"dp": mate}).start()

        return 0

    lax.fori_loop(0, 4, block, 0)
    tok[z] = heads[z]
    for i in range(1, 4):
        c = remote(wv.at[dp], wv.at[dp], wss.at[i], wsr.at[i], {"dp": mate})
        pending.append(c)
        c.wait_recv()
    mates[0].wait_recv()
    loads["r"].wait()
    for t in range(3):
        c = remote(heads.at[t], tok.at[t], hs.at[t], hr.at[t], sp_of(z + 1, x))
        pending.append(c)
        c.wait_recv()
    for c in pending:
        c.wait_send()

    sq = None
    for nb in range(4):
        cols = slice(nb * 512, (nb + 1) * 512)
        acc = None
        for k in range(4):
            w = wv[2 * k:2 * k + 2, :, :, cols].reshape(512, 512)
            part = jnp.dot(tok[k], w, preferred_element_type=F32)
            acc = part if acc is None else acc + part
        u = (rv[:, cols].astype(F32) + acc).astype(BF)
        u_ref[:, cols] = u
        wide = u.astype(F32)
        part = jnp.sum(wide * wide, axis=-1, keepdims=True)
        sq = part if sq is None else sq + part
    inv = lax.rsqrt(sq / 2048.0 + EPSILON)
    for j in range(16):
        cols = slice(j * HD, (j + 1) * HD)
        n3[:, j, :] = u_ref[:, cols].astype(F32) * inv * ng_ref[:, cols]

    def narrow(t, _):
        rows = pl.ds(t * 8, 8)
        n_ref[rows] = n3[rows].astype(BF)
        return 0

    lax.fori_loop(0, TOK // 8, narrow, 0)


GROUPS = 4
PER = N_DEV // GROUPS
STEP = 37


def moe_kernel(slot_ref, tgt_ref, wt_ref, n_ref, u_ref, wg_hbm, wu_hbm, wd_hbm, o_ref,
               wg, wu, wd, rows, came, y, ret, w3, xs, act, c3, wsem, ss, rs, ys, yr):
    me = lax.axis_index("sp") * 8 + lax.axis_index("dp")
    bar = pltpu.get_barrier_semaphore()
    n = PER * CAP

    def dev(p):
        return {"sp": p // 8, "dp": lax.rem(p, 8)}

    def ahead(i):
        return lax.rem(me + i * STEP, N_DEV)

    def behind(i):
        return lax.rem(me + i * (N_DEV - STEP), N_DEV)

    def sig(i, _):
        pl.semaphore_signal(bar, inc=1, device_id=dev(lax.rem(me + i, N_DEV)), device_id_type=MESH)
        return 0

    lax.fori_loop(1, N_DEV, sig, 0)
    loads = []
    for k in range(4):
        for src, dst in ((wg_hbm.at[:, k * 256:(k + 1) * 256], wg.at[k]), (wu_hbm.at[:, k * 256:(k + 1) * 256], wu.at[k]),
                         (wd_hbm.at[:, k * 512:(k + 1) * 512], wd.at[k])):
            c = pltpu.make_async_copy(src, dst, wsem.at[len(loads)])
            c.start()
            loads.append(c)

    def pick(i, _):
        p = ahead(i)
        for r in range(CAP):
            rows[i, r] = n_ref[slot_ref[0, p * CAP + r]]
        return 0

    def send(i, _):
        p = ahead(i)
        pltpu.make_async_remote_copy(rows.at[i], came.at[i], ss, rs.at[i // PER], device_id=dev(p), device_id_type=MESH).start()
        return 0

    lax.fori_loop(0, PER, pick, 0)
    came[0] = rows[0]
    pl.semaphore_wait(bar, N_DEV - 1)
    lax.fori_loop(1, PER, send, 0)
    for g in range(1, GROUPS):
        lax.fori_loop(g * PER, (g + 1) * PER, pick, 0)
        lax.fori_loop(g * PER, (g + 1) * PER, send, 0)
    for c in loads:
        c.wait()

    def group(g, _):
        base = g * PER

        def arrived(first, count, sem):
            part = pl.ds(first, count)
            pltpu.make_async_remote_copy(rows.at[part], came.at[part], ss, sem, device_id=dev(me), device_id_type=MESH).wait_recv()

        @pl.when(g == 0)
        def _():
            arrived(1, PER - 1, rs.at[0])

        @pl.when(g > 0)
        def _():
            arrived(base, PER, rs.at[g])

        def widen(t, _):
            for r in range(CAP):
                w3[t * CAP + r] = came[base + t, r].astype(F32)
            return 0

        lax.fori_loop(0, PER, widen, 0)
        for j in range(16):
            xs[:, j * HD:(j + 1) * HD] = w3[:, j, :].astype(BF)

        def up(k, _):
            x = xs[...]
            a = jnp.minimum(jnp.dot(x, wg[k], preferred_element_type=F32), LIMIT)
            b = jnp.clip(jnp.dot(x, wu[k], preferred_element_type=F32), -LIMIT, LIMIT)
            act[k] = (a * jax.nn.sigmoid(SLOPE * a) * (b + 1.0)).astype(BF)
            return 0

        lax.fori_loop(0, 4, up, 0)

        for k in range(4):
            d = jnp.dot(act[0], wd[k, 0:256, :], preferred_element_type=F32)
            for m in range(1, 4):
                d = d + jnp.dot(act[m], wd[k, m * 256:(m + 1) * 256, :], preferred_element_type=F32)
            for j in range(4):
                w3[:, k * 4 + j, :] = d[:, j * HD:(j + 1) * HD]

        def narrow(t, _):
            for r in range(CAP):
                y[base + t, r] = w3[t * CAP + r].astype(BF)
            return 0

        lax.fori_loop(0, PER, narrow, 0)

        def answer(t, _):
            i = base + t
            pltpu.make_async_remote_copy(y.at[i], ret.at[me], ys, yr, device_id=dev(behind(i)), device_id_type=MESH).start()
            return 0

        @pl.when(g == 0)
        def _():
            ret[me] = y[0]
            lax.fori_loop(1, PER, answer, 0)

        @pl.when(g > 0)
        def _():
            lax.fori_loop(0, PER, answer, 0)

        return 0

    lax.fori_loop(0, GROUPS, group, 0)
    rest = pl.ds(0, N_DEV - 1)
    pltpu.make_async_remote_copy(y.at[rest], ret.at[rest], ys, yr, device_id=dev(me), device_id_type=MESH).wait()
    pltpu.make_async_remote_copy(rows.at[rest], came.at[rest], ss, rs.at[0], device_id=dev(me), device_id_type=MESH).wait_send()

    def token(t, _):
        for h in range(4):
            q = t * 4 + h
            i0, i1 = tgt_ref[0, 2 * q], tgt_ref[0, 2 * q + 1]
            a = ret[i0 // CAP, lax.rem(i0, CAP)].astype(F32) * wt_ref[0, 2 * q]
            b = ret[i1 // CAP, lax.rem(i1, CAP)].astype(F32) * wt_ref[0, 2 * q + 1]
            c3[q] = a + b
        return 0

    lax.fori_loop(0, TOK // 4, token, 0)
    for j in range(16):
        cols = slice(j * HD, (j + 1) * HD)
        o_ref[:, cols] = (u_ref[:, cols].astype(F32) + c3[:, j, :]).astype(BF)


def full(shape):
    return pl.BlockSpec(shape, lambda *i: (0,) * len(shape))


def per_device(resid, query, keys, values, q_gain, k_gain, out_weight, norm_gain, route_ids, route_weight,
               expert_gate, expert_up, expert_down):
    sds = jax.ShapeDtypeStruct
    sem = pltpu.SemaphoreType.DMA
    places = lax.axis_index("sp") * TOK + jnp.arange(TOK, dtype=jnp.int32)
    cosine, sine = turn_tables(places)
    ANY = pl.BlockSpec(memory_space=pl.ANY)
    V = pltpu.VMEM
    updated, rows, target, slots = pl.pallas_call(
        front_kernel,
        out_shape=(sds((TOK, 2048), BF), sds((TOK, 16, HD), BF), sds((1, 2 * TOK), jnp.int32),
                   sds((1, N_DEV * CAP), jnp.int32)),
        in_specs=[ANY] * 7 + [VM] * 4, out_specs=(VM,) * 4,
        scratch_shapes=[V((TOK, 2048), BF), V((TOK, 512), BF), V((TOK, 512), BF), V((TOK, 2048), BF),
                        V((8, 2, 128, 2048), BF), V((TOK, HD), F32), V((TOK, HD), F32),
                        V((4, TOK, 512), BF), V((4, 2, TOK, HD), BF), V((4, TOK, 512), BF), V((4, 4, 2, TOK, HD), BF),
                        V((4096, 256), BF), V((4, TOK, 512), BF), V((4, TOK, 512), BF), V((TOK, 16, HD), F32),
                        sem((7,)), sem((3,)), sem((3,)), sem((3,)), sem((3,)), sem((2, 4)), sem((2, 4)), sem((4,)), sem((4,)),
                        sem((3,)), sem((3,)), sem((2, 2)), sem((2, 2)), sem((2,)), sem((2,)), sem((4,)), sem((4,))],
        compiler_params=params(56 * MB, cid=0), name="front",
    )(query[0], keys[0], values[0], resid[0], out_weight.reshape(2, 128, 2048), cosine, sine,
      q_gain[None], k_gain[None], norm_gain[None], route_ids[0].reshape(1, 2 * TOK))
    tiles = pltpu.VMEM((N_DEV, CAP, 16, HD), BF)
    n = PER * CAP
    out = pl.pallas_call(
        moe_kernel,
        out_shape=sds((TOK, 2048), BF),
        in_specs=[SM, SM, SM, VM, VM] + [pl.BlockSpec(memory_space=pl.ANY)] * 3, out_specs=VM,
        scratch_shapes=[pltpu.VMEM((4, 2048, 256), BF), pltpu.VMEM((4, 2048, 256), BF), pltpu.VMEM((4, 1024, 512), BF),
                        tiles, tiles, tiles, tiles, pltpu.VMEM((n, 16, HD), F32), pltpu.VMEM((n, 2048), BF),
                        pltpu.VMEM((4, n, 256), BF), pltpu.VMEM((TOK, 16, HD), F32),
                        sem((12,)), sem, sem((GROUPS,)), sem, sem],
        compiler_params=params(cid=1), name="moe",
    )(slots, target, route_weight[0].reshape(1, 2 * TOK), rows, updated, expert_gate[0], expert_up[0], expert_down[0])
    return out[None]


def solution(mesh):
    placed = (
        P("dp", "sp", None),
        P("dp", "sp", None),
        P("dp", "sp", None),
        P("dp", "sp", None),
        P(),
        P(),
        P("dp", None),
        P(),
        P("dp", "sp", None),
        P("dp", "sp", None),
        P(("sp", "dp"), None, None),
        P(("sp", "dp"), None, None),
        P(("sp", "dp"), None, None),
    )
    return jax.shard_map(
        per_device, mesh=mesh, in_specs=placed, out_specs=P("dp", "sp", None), check_vma=False
    )
```

time: 190 us -> 157 us (0.83)
  Pallas kernels: 166 us -> 145 us
  between operations: 13.6 us -> 0.06 us
    pallas_call x5 -> x1, Pallas kernels: 80.7 us -> 60.1 us  [per_device(): pl.pallas_call(front_kernel, out_shape=(sds((TOK, 2048), BF), sds((TOK, 1...]
    unnamed x19 -> x11, local copies, waits for them, and re-layouts: 6.36 us -> 6.39 us
  transfers between devices with their start and end apart: 1 -> 0, of which waited for: 0 -> 0; matrix products, arithmetic and copies ran while one was open for 1% -> 0% of each run, Pallas kernels for 39% -> 0%
where the time goes in v3:
time: 157 us; the launch traced here: 153 us
  Pallas kernels  145 us (92%)
  local copies, waits for them, and re-layouts  7.27 us (5%)
    pallas_call x1, Pallas kernels, per_device(): pl.pallas_call(moe_kernel, out_shape=sds((TOK, 2048), BF), in_specs=[SM,...  84.7 us
    pallas_call x1, Pallas kernels, per_device(): pl.pallas_call(front_kernel, out_shape=(sds((TOK, 2048), BF), sds((TOK, 1...  60.1 us
    unnamed x11, local copies, waits for them, and re-layouts  6.39 us

profile of v3, /device:TPU:6, one launch (start us, length us, event | category | flops | bytes accessed | tf_op | source)
XLA Modules:
  0.0 153.4 jit_solution(18378243273727464172)
XLA Ops:
  0.0 0.8 copy.16
  0.8 0.7 reshape_squeeze.6.ids_ref
  1.6 0.8 copy.17
  2.4 0.1 reshape_squeeze.7.wt_ref
  2.5 1.3 sine_multiply_fusion
  3.8 60.1 %front.1 = (bf16[256,2048]{1,0:T(8,128)(2,1)}, bf16[256,16,128]{2,1,0:T(8,128)(2,1)}, s32[1,512]{1,0:T(1,128)}, s32[1,768]{1,0:T(1,128)}) custom-call(bf16[256,2048]{1,0:T(8,128)(2,1)} %bitcast.16, bf16[256,512]{1,0:T(8,128)(2,1)} %bitcast.19, bf16[256,512]{1,0:T(8,128)(2,1)} %bitcast.20, bf16[256,2048]{1,0:T(8,128)(2,1)} %bitcast.17, ...), custom_call_target="tpu_custom_call" | custom-call | tf_op jit(solution)/shard_map/front/pallas_call | solution.py:420
  64.0 0.0 copy-start
  64.0 1.2 copy-done
  65.2 0.0 copy-start.1
  65.2 1.2 copy-done.1
  66.4 0.0 copy-start.2
  66.4 0.7 copy-done.2
  67.1 0.0 copy-start.3
  67.1 0.7 copy-done.3
  67.8 84.7 %moe.1 = bf16[256,2048]{1,0:T(8,128)(2,1)S(1)} custom-call(s32[1,768]{1,0:T(1,128)S(1)} %copy-done.2, s32[1,512]{1,0:T(1,128)S(1)} %copy-done.3, f32[1,512]{1,0:T(1,128)S(1)} %reshape_squeeze.7.wt_ref, bf16[256,16,128]{2,1,0:T(8,128)(2,1)S(1)} %copy-done.1, bf16[256,2048]{1,0:T(8,128)(2,1)S(1)} %copy-done, bf16[2048,1024]{1,0:T(8,128)(2,1)} %bitcast.13, ...), custom_call_target="tpu_custom_call" | custom-call | tf_op jit(solution)/shard_map/moe/pallas_call | solution.py:436
  152.5 1.0 copy.19
  (3 shorter events, 0.0 us)
Async XLA Ops:
  64.0 1.2 copy-start
  65.2 1.2 copy-start.1
  66.4 0.7 copy-start.2
  67.1 0.7 copy-start.3

commit v4 on v3

v4 whole, which is shorter than its diff:
```python
import functools
import jax
import jax.numpy as jnp
from jax import lax
from jax.experimental import pallas as pl
from jax.experimental.pallas import tpu as pltpu
from jax.sharding import PartitionSpec as P

GRID_W = 64
EPSILON = 1e-06
THETA = 10000.0
LIMIT = 7.0
SLOPE = 1.702
LOG2E = 1.4426950408889634
HD = 128
TOK = 256
ZN = 4
XN = 4
N_DEV = 128
GROUPS = 4
PER = N_DEV // GROUPS
STEP = 37
CAP = 6
BF = jnp.bfloat16
F32 = jnp.float32
MESH = pl.DeviceIdType.MESH
VM = pl.BlockSpec(memory_space=pltpu.VMEM)
SM = pl.BlockSpec(memory_space=pltpu.SMEM)
MB = 1 << 20
LIM = 56


def params(limit=48 * MB, cid=None, **kw):
    if cid is not None:
        kw.update(collective_id=cid, has_side_effects=True)
    return pltpu.CompilerParams(vmem_limit_bytes=limit, **kw)


def turn_tables(sp):
    lane = jnp.arange(HD, dtype=jnp.int32)
    inverse = THETA ** (-(lane % 32).astype(F32) / 32)
    at = jnp.arange(GRID_W + 8, dtype=jnp.int32)
    place = jnp.where(at < GRID_W, at, sp * (TOK // GRID_W) + at - GRID_W)
    angles = place.astype(F32)[:, None] * inverse[None, :]
    sign = jnp.where(lane % 64 < 32, -1.0, 1.0)
    return jnp.cos(angles), jnp.sin(angles) * sign[None, :]


def per_token(table):
    lane = lax.broadcasted_iota(jnp.int32, (GRID_W, HD), 1)
    return jnp.concatenate(
        [jnp.where(lane < 64, table[GRID_W + b:GRID_W + b + 1, :], table[:GRID_W, :]) for b in range(TOK // GRID_W)], axis=0)


def turn_head(x, gain, cosine, sine, first):
    x = x.astype(F32)
    x = x * lax.rsqrt(jnp.mean(x * x, axis=-1, keepdims=True) + EPSILON) * gain
    other = jnp.where(first, pltpu.roll(x, HD - 32, 1), pltpu.roll(x, 32, 1))
    return (x * cosine + other * sine).astype(BF)


def sp_of(z, x):
    return {"sp": lax.rem(z, ZN) * XN + lax.rem(x, XN)}


def dp_of(y, c):
    return lax.rem(y, 4) * 2 + lax.rem(c, 2)


def route_tables(ids_ref, tgt_ref, slot_ref):
    n = 2 * TOK
    row = jnp.concatenate([ids_ref[0:1, :], ids_ref[1:2, :]], axis=1).astype(F32)
    ia = lax.broadcasted_iota(jnp.int32, (n, n), 0)
    ib = lax.broadcasted_iota(jnp.int32, (n, n), 1)
    col = jnp.sum(jnp.where(ia == ib, row, 0.0), axis=1, keepdims=True)
    same = col == row
    before = jnp.sum(jnp.where(same & (ia < ib), 1.0, 0.0), axis=0, keepdims=True)
    tgt_ref[...] = (row * CAP + before).astype(jnp.int32)
    before_c = jnp.sum(jnp.where(same & (ib < ia), 1.0, 0.0), axis=1, keepdims=True)
    target = (col * CAP + before_c).astype(jnp.int32)
    slots = lax.broadcasted_iota(jnp.int32, (n, N_DEV * CAP), 1)
    token = (lax.broadcasted_iota(jnp.int32, (n, N_DEV * CAP), 0) % TOK).astype(F32)
    slot_ref[...] = jnp.sum(jnp.where(target == slots, token, 0.0), axis=0, keepdims=True).astype(jnp.int32)


STEP_BLOCK = (3, 0, 1, 2, 0, 0, 1, 1, 0, 1, 2, 2, 2, 3, 3, 3)
STEP_QUARTER = (0, 0, 0, 0, 1, 3, 1, 3, 2, 2, 1, 3, 2, 1, 3, 2)


def step_entry(table, i):
    return sum(v * ((16 - lax.rem(i + 16 - k, 16)) // 16) for k, v in enumerate(table) if v)


def attend(q, kvr, ve, quarter, acc_ref, top_ref):
    scale = HD ** -0.5 * LOG2E
    q = jnp.concatenate([q[:, h * HD:(h + 1) * HD] for h in range(4)], axis=0)
    m, acc = jnp.max(top_ref[...], axis=-1, keepdims=True), acc_ref[...]
    for c in range(4):
        k = kvr[quarter, c, 0]
        s = lax.dot_general(q, k, (((1,), (1,)), ((), ())), preferred_element_type=F32)
        m_new = jnp.maximum(m, jnp.max(s, axis=-1, keepdims=True) * scale)
        p = jnp.exp2(s * scale - m_new).astype(BF)
        acc = acc * jnp.exp2(m - m_new) + jnp.dot(p, ve[quarter, c * TOK:(c + 1) * TOK, :], preferred_element_type=F32)
        m = m_new
    acc_ref[...] = acc
    top_ref[...] = jnp.broadcast_to(m, top_ref.shape)


def layer_kernel(q_hbm, k_hbm, v_hbm, r_hbm, w_hbm, wg_hbm, wu_hbm, wd_hbm, cos_ref, sin_ref, qg_ref, kg_ref, ng_ref, ids_ref, wt_ref,
                 o_ref,
                 qv, kx, vx, rv, wv, qs, kvs, qr, kvr, ve, heads, tok, n3, acc, tops, tgt_v, slot_v, tgt_s, slot_s,
                 u_ref, n_ref, wd, rows, came, ret, w3, xs_v, act,
                 ls, tsem, zks, zkr, zqs, zqr, xs, xr, fs, fr, hs, hr, w1s, w1r, w2s, w2r, wss, wsr, wsem, ss, rs, ys, yr, in_x, in_dp):
    sp, dp = lax.axis_index("sp"), lax.axis_index("dp")
    z, x = sp // XN, lax.rem(sp, XN)
    yy, core = dp // 2, lax.rem(dp, 2)
    me = sp * 8 + dp
    above, below, mate = dp_of(yy + 1, core), dp_of(yy + 3, core), dp_of(yy, core + 1)
    far_shard = dp_of(yy + 2, core)
    bar = pltpu.get_barrier_semaphore()

    def dev(p):
        return {"sp": p // 8, "dp": lax.rem(p, 8)}

    loads = {}
    for i, (name, src, dst) in enumerate((("k", k_hbm, kx), ("v", v_hbm, vx), ("q", q_hbm, qv), ("r", r_hbm, rv))):
        loads[name] = pltpu.make_async_copy(src, dst, ls.at[i])
        loads[name].start()

    w_loads = [pltpu.make_async_copy(w_hbm.at[:, nb * 512:(nb + 1) * 512], wv.at[nb, pl.ds(pl.multiple_of(dp * 256, 256), 256), :], ls.at[4 + nb])
               for nb in range(4)]
    for c in w_loads:
        c.start()

    def shard(p, half=None):
        if half is None:
            return wv.at[:, pl.ds(pl.multiple_of(p * 256, 256), 256), :]
        return wv.at[:, pl.ds(pl.multiple_of(p * 256 + half * 128, 128), 128), :]

    for d in (1, 2, 3):
        pl.semaphore_signal(bar, inc=1, device_id=sp_of(z + d, x), device_id_type=MESH)
        pl.semaphore_signal(bar, inc=1, device_id=sp_of(z, x + d), device_id_type=MESH)
    for d in range(1, 8):
        pl.semaphore_signal(bar, inc=1, device_id={"dp": lax.rem(dp + d, 8)}, device_id_type=MESH)
    weights = []
    for k in range(4):
        for src, dst in ((wg_hbm.at[:, k * 256:(k + 1) * 256], wv.at[k, :, 0:256]), (wu_hbm.at[:, k * 256:(k + 1) * 256], wv.at[k, :, 256:512]),
                         (wd_hbm.at[:, k * 512:(k + 1) * 512], wd.at[k])):
            weights.append(pltpu.make_async_copy(src, dst, wsem.at[len(weights)]))
    pending = []

    def remote(src, dst, ssem, rsem, dev):
        return pltpu.make_async_remote_copy(src, dst, ssem, rsem, device_id=dev, device_id_type=MESH)

    def send(src, dst, ssem, rsem, dev):
        c = remote(src, dst, ssem, rsem, dev)
        c.start()
        pending.append(c)
        return c

    pl.semaphore_wait(bar, 13)
    for d in (1, 2, 3):
        pl.semaphore_signal(in_x, inc=1, device_id=sp_of(z, x + d), device_id_type=MESH)
    for c in w_loads:
        c.wait()
    near_w = {}
    for half in (0, 1):
        for s, p in ((0, above), (1, below)):
            h = half if s == 0 else 1 - half
            near_w[s, h] = send(shard(dp, h), shard(dp, h), w1s.at[s, h], w1r.at[s, h], {"dp": p})
    mates = [send(shard(dp), shard(dp), wss.at[0], wsr.at[0], {"dp": mate})]
    first = lax.broadcasted_iota(jnp.int32, (TOK, HD), 1) % 64 < 32
    cosine, sine = per_token(cos_ref[...]), per_token(sin_ref[...])
    loads["k"].wait()
    loads["v"].wait()
    for h in range(4):
        kvs[h, 0] = turn_head(kx[:, h * HD:(h + 1) * HD], kg_ref[...], cosine, sine, first)
        kvs[h, 1] = vx[:, h * HD:(h + 1) * HD]
    zk = {}
    for d in (1, 3, 2):
        zk[d] = send(kvs.at[lax.rem(z + d, ZN)], kvr.at[x, z], zks.at[d - 1], zkr.at[d - 1], sp_of(z + d, x))
    kvr[x, z] = kvs[z]

    def gather(d):
        chunk = lax.rem(z + ZN - d, ZN)
        return [send(kvr.at[x, chunk], kvr.at[x, chunk], xs.at[s, d], xr.at[s, d], sp_of(z, x + (1, 3)[s])) for s in (0, 1)]

    near = {0: gather(0)}
    loads["q"].wait()

    def turn_query(d):
        zz = lax.rem(z + d, ZN)
        for h in range(4):
            cols = pl.ds(pl.multiple_of(zz * 512 + h * HD, HD), HD)
            val = turn_head(qv[:, cols], qg_ref[...], cosine, sine, first)
            if d:
                qs[zz, :, h * HD:(h + 1) * HD] = val
            else:
                qr[zz, :, h * HD:(h + 1) * HD] = val
        return zz

    for d in (3, 2, 1):
        zz = turn_query(d)
        send(qs.at[zz], qr.at[z], zqs.at[d - 1], zqr.at[d - 1], sp_of(z + d, x))
    def far_copy(d):
        chunk = lax.rem(z + ZN - d, ZN)
        s = 0 if d in (0, 1) else 1
        came_x = lax.rem(x + (3, 1)[s], XN)
        return remote(kvr.at[came_x, chunk], kvr.at[came_x, chunk], fs.at[d], fr.at[d], sp_of(z, x + (1, 3)[s]))

    def forward(d):
        near[d][0 if d in (0, 1) else 1].wait_recv()
        far_copy(d).start()

    far_w = [remote(shard(below, 0), shard(below, 0), w2s.at[0], w2r.at[0], {"dp": above}),
             remote(shard(above, 1), shard(above, 1), w2s.at[1], w2r.at[1], {"dp": below})]
    for c in weights[2::3]:
        c.start()
    route_tables(ids_ref, tgt_v, slot_v)
    tables = [pltpu.make_async_copy(tgt_v, tgt_s, tsem.at[0]), pltpu.make_async_copy(slot_v, slot_s, tsem.at[1])]
    for c in tables:
        c.start()
    pending += far_w + [far_copy(d) for d in range(4)]
    turn_query(0)
    pl.semaphore_wait(in_x, 3)
    for d in range(1, 8):
        pl.semaphore_signal(in_dp, inc=1, device_id={"dp": lax.rem(dp + d, 8)}, device_id_type=MESH)
    zk[1].wait_recv()
    near[1] = gather(1)
    zk[3].wait_recv()
    near[3] = gather(3)
    acc[...] = jnp.zeros_like(acc)
    tops[...] = jnp.full_like(tops, -jnp.inf)
    lane = lax.broadcasted_iota(jnp.int32, (1024, HD), 1)
    for c in range(4):
        ve[c, :, HD:] = jnp.where(lane == 0, 1.0, 0.0).astype(BF)
    zk[2].wait_recv()
    near[2] = gather(2)
    forward(0)

    def value_quarter(quarter):
        ve[quarter, :, :HD] = kvr[quarter, :, 1].reshape(1024, HD)

    value_quarter(x)

    def step(i, _):
        t, turn = step_entry(STEP_BLOCK, i), step_entry(STEP_QUARTER, i)
        a, quarter = lax.rem(z + 1 + t, ZN), lax.rem(x + ZN - turn, XN)

        @pl.when((i > 0) & (i < 4))
        def _():
            remote(qs.at[a], qr.at[a], zqs.at[2 - t], zqr.at[2 - t], sp_of(a, x)).wait_recv()

        @pl.when(i == 1)
        def _():
            forward(1)

        @pl.when(i == 3)
        def _():
            forward(3)

        @pl.when(i == 4)
        def _():
            forward(2)
            near[2][0].wait_recv()
            near[3][0].wait_recv()
            value_quarter(quarter)

        @pl.when(i == 5)
        def _():
            near[0][1].wait_recv()
            near[1][1].wait_recv()
            value_quarter(quarter)

        @pl.when(i == 6)
        def _():
            near_w[0, 0].wait_recv()
            remote(shard(below, 0), shard(below, 0), w2s.at[0], w2r.at[0], {"dp": above}).start()
            near_w[1, 1].wait_recv()
            remote(shard(above, 1), shard(above, 1), w2s.at[1], w2r.at[1], {"dp": below}).start()

        @pl.when(i == 8)
        def _():
            for d in range(4):
                far_copy(d).wait_recv()
            value_quarter(quarter)

        attend(qr[a], kvr, ve, quarter, acc.at[t], tops.at[t])

        @pl.when(turn == 2)
        def _():
            done = acc[t]
            out = (done[:, :HD] / done[:, HD:HD + 1]).astype(BF)
            for h in range(4):
                heads[a, :, h * HD:(h + 1) * HD] = out[h * TOK:(h + 1) * TOK]

        @pl.when((turn == 2) & (t < 3))
        def _():
            remote(heads.at[a], tok.at[z], hs.at[t], hr.at[t], sp_of(a, x)).start()

        @pl.when(i == 11)
        def _():
            near_w[0, 1].wait_recv()
            remote(shard(below), shard(below), wss.at[1], wsr.at[1], {"dp": mate}).start()
            near_w[1, 0].wait_recv()
            remote(shard(above), shard(above), wss.at[2], wsr.at[2], {"dp": mate}).start()

        return 0

    lax.fori_loop(0, 16, step, 0)
    for c in far_w:
        c.wait_recv()
    remote(shard(far_shard), shard(far_shard), wss.at[3], wsr.at[3], {"dp": mate}).start()
    tok[z] = heads[z]
    for i in range(1, 4):
        c = remote(shard(dp), shard(dp), wss.at[i], wsr.at[i], {"dp": mate})
        pending.append(c)
        c.wait_recv()
    mates[0].wait_recv()
    loads["r"].wait()
    for t in range(3):
        c = remote(heads.at[t], tok.at[t], hs.at[t], hr.at[t], sp_of(z + 1, x))
        pending.append(c)
        c.wait_recv()
    for c in pending:
        c.wait_send()

    sq = None
    for nb in range(4):
        cols = slice(nb * 512, (nb + 1) * 512)
        acc = None
        for k in range(4):
            part = jnp.dot(tok[k], wv[nb, k * 512:(k + 1) * 512, :], preferred_element_type=F32)
            acc = part if acc is None else acc + part
        u = (rv[:, cols].astype(F32) + acc).astype(BF)
        u_ref[:, cols] = u
        wide = u.astype(F32)
        part = jnp.sum(wide * wide, axis=-1, keepdims=True)
        sq = part if sq is None else sq + part
    for i, c in enumerate(weights):
        if i % 3 < 2:
            c.start()
    inv = lax.rsqrt(sq / 2048.0 + EPSILON)
    for j in range(16):
        cols = slice(j * HD, (j + 1) * HD)
        n3[:, j, :] = u_ref[:, cols].astype(F32) * inv * ng_ref[:, cols]

    def narrow(t, _):
        rows = pl.ds(t * 8, 8)
        n_ref[rows] = n3[rows].astype(BF)
        return 0

    lax.fori_loop(0, TOK // 8, narrow, 0)

    n = PER * CAP

    def ahead(i):
        return lax.rem(me + i * STEP, N_DEV)

    def behind(i):
        return lax.rem(me + i * (N_DEV - STEP), N_DEV)

    for c in tables:
        c.wait()

    def pick(i, _):
        p = ahead(i)
        for r in range(CAP):
            rows[i, r] = n_ref[jnp.clip(slot_s[0, p * CAP + r], 0, TOK - 1)]
        return 0

    def send_row(i, _):
        p = ahead(i)
        pltpu.make_async_remote_copy(rows.at[i], came.at[i], ss, rs.at[i // PER], device_id=dev(p), device_id_type=MESH).start()
        return 0

    lax.fori_loop(0, PER, pick, 0)
    came[0] = rows[0]
    pl.semaphore_wait(in_dp, 7)
    lax.fori_loop(1, PER, send_row, 0)
    for g in range(1, GROUPS):
        lax.fori_loop(g * PER, (g + 1) * PER, pick, 0)
        lax.fori_loop(g * PER, (g + 1) * PER, send_row, 0)
    for c in weights:
        c.wait()

    def group(g, _):
        base = g * PER

        def arrived(first, count, sem):
            part = pl.ds(first, count)
            pltpu.make_async_remote_copy(rows.at[part], came.at[part], ss, sem, device_id=dev(me), device_id_type=MESH).wait_recv()

        @pl.when(g == 0)
        def _():
            arrived(1, PER - 1, rs.at[0])

        @pl.when(g > 0)
        def _():
            arrived(base, PER, rs.at[g])

        def widen(t, _):
            for r in range(CAP):
                w3[t * CAP + r] = came[base + t, r].astype(F32)
            return 0

        lax.fori_loop(0, PER, widen, 0)
        for j in range(16):
            xs_v[:, j * HD:(j + 1) * HD] = w3[:, j, :].astype(BF)

        def up(k, _):
            xb = xs_v[...]
            a = jnp.minimum(jnp.dot(xb, wv[k, :, 0:256], preferred_element_type=F32), LIMIT)
            b = jnp.clip(jnp.dot(xb, wv[k, :, 256:512], preferred_element_type=F32), -LIMIT, LIMIT)
            act[k] = (a * jax.nn.sigmoid(SLOPE * a) * (b + 1.0)).astype(BF)
            return 0

        lax.fori_loop(0, 4, up, 0)

        for k in range(4):
            d = jnp.dot(act[0], wd[k, 0:256, :], preferred_element_type=F32)
            for m in range(1, 4):
                d = d + jnp.dot(act[m], wd[k, m * 256:(m + 1) * 256, :], preferred_element_type=F32)
            for j in range(4):
                w3[:, k * 4 + j, :] = d[:, j * HD:(j + 1) * HD]

        def narrow(t, _):
            for r in range(CAP):
                came[base + t, r] = w3[t * CAP + r].astype(BF)
            return 0

        lax.fori_loop(0, PER, narrow, 0)

        def answer(t, _):
            i = base + t
            pltpu.make_async_remote_copy(came.at[i], ret.at[me], ys, yr, device_id=dev(behind(i)), device_id_type=MESH).start()
            return 0

        @pl.when(g == 0)
        def _():
            ret[me] = came[0]
            lax.fori_loop(1, PER, answer, 0)

        @pl.when(g > 0)
        def _():
            lax.fori_loop(0, PER, answer, 0)

        return 0

    lax.fori_loop(0, GROUPS, group, 0)
    rest = pl.ds(0, N_DEV - 1)
    pltpu.make_async_remote_copy(came.at[rest], ret.at[rest], ys, yr, device_id=dev(me), device_id_type=MESH).wait()
    pltpu.make_async_remote_copy(rows.at[rest], came.at[rest], ss, rs.at[0], device_id=dev(me), device_id_type=MESH).wait_send()

    def token(t, _):
        for h in range(4):
            q = t * 4 + h
            i0, i1 = (jnp.clip(tgt_s[0, k], 0, N_DEV * CAP - 1) for k in (q, TOK + q))
            a = ret[i0 // CAP, lax.rem(i0, CAP)].astype(F32) * wt_ref[0, q]
            b = ret[i1 // CAP, lax.rem(i1, CAP)].astype(F32) * wt_ref[1, q]
            n3[q] = a + b
        return 0

    lax.fori_loop(0, TOK // 4, token, 0)
    for j in range(16):
        cols = slice(j * HD, (j + 1) * HD)
        o_ref[:, cols] = (u_ref[:, cols].astype(F32) + n3[:, j, :]).astype(BF)


def full(shape):
    return pl.BlockSpec(shape, lambda *i: (0,) * len(shape))


def per_device(resid, query, keys, values, q_gain, k_gain, out_weight, norm_gain, route_ids, route_weight,
               expert_gate, expert_up, expert_down):
    sds = jax.ShapeDtypeStruct
    sem = pltpu.SemaphoreType.DMA
    cosine, sine = turn_tables(lax.axis_index("sp"))
    ANY = pl.BlockSpec(memory_space=pl.ANY)
    V = pltpu.VMEM
    n = PER * CAP
    tiles = V((N_DEV, CAP, 16, HD), BF)
    out = pl.pallas_call(
        layer_kernel,
        out_shape=sds((TOK, 2048), BF),
        in_specs=[ANY] * 8 + [VM] * 6 + [SM], out_specs=VM,
        scratch_shapes=[V((TOK, 2048), BF), V((TOK, 512), BF), V((TOK, 512), BF), V((TOK, 2048), BF), V((4, 2048, 512), BF),
                        V((4, TOK, 512), BF), V((4, 2, TOK, HD), BF), V((4, TOK, 512), BF), V((4, 4, 2, TOK, HD), BF),
                        V((4, 1024, 256), BF), V((4, TOK, 512), BF), V((4, TOK, 512), BF), V((TOK, 16, HD), F32),
                        V((4, 1024, 256), F32), V((4, 1024, HD), F32), V((1, 2 * TOK), jnp.int32), V((1, N_DEV * CAP), jnp.int32),
                        pltpu.SMEM((1, 2 * TOK), jnp.int32), pltpu.SMEM((1, N_DEV * CAP), jnp.int32),
                        V((TOK, 2048), BF), V((TOK, 16, HD), BF), V((4, 1024, 512), BF),
                        tiles, tiles, tiles, V((n, 16, HD), F32), V((n, 2048), BF), V((4, n, 256), BF),
                        sem((8,)), sem((2,)), sem((3,)), sem((3,)), sem((3,)), sem((3,)), sem((2, 4)), sem((2, 4)), sem((4,)), sem((4,)),
                        sem((3,)), sem((3,)), sem((2, 2)), sem((2, 2)), sem((2,)), sem((2,)), sem((4,)), sem((4,)),
                        sem((12,)), sem, sem((GROUPS,)), sem, sem,
                        pltpu.SemaphoreType.REGULAR, pltpu.SemaphoreType.REGULAR],
        compiler_params=params(LIM * MB, cid=0), name="layer",
    )(query[0], keys[0], values[0], resid[0], out_weight, expert_gate[0], expert_up[0], expert_down[0],
      cosine, sine, q_gain[None], k_gain[None], norm_gain[None], route_ids[0].T, route_weight[0].T)
    return out[None]


def solution(mesh):
    placed = (
        P("dp", "sp", None),
        P("dp", "sp", None),
        P("dp", "sp", None),
        P("dp", "sp", None),
        P(),
        P(),
        P("dp", None),
        P(),
        P("dp", "sp", None),
        P("dp", "sp", None),
        P(("sp", "dp"), None, None),
        P(("sp", "dp"), None, None),
        P(("sp", "dp"), None, None),
    )
    return jax.shard_map(
        per_device, mesh=mesh, in_specs=placed, out_specs=P("dp", "sp", None), check_vma=False
    )
```

time: 157 us -> 145 us (0.924); the launches traced: 153 us -> 143 us
  Pallas kernels: 145 us -> 140 us
  local copies, waits for them, and re-layouts: 7.27 us -> 2.3 us
    pallas_call x2 -> x1, Pallas kernels: 145 us -> 140 us  [per_device(): pl.pallas_call(layer_kernel, out_shape=sds((TOK, 2048), BF), in_specs=[AN...]
    unnamed x11 -> x1, local copies, waits for them, and re-layouts: 6.39 us -> 2.3 us
where the time goes in v4:
time: 145 us; the launch traced here: 143 us
  Pallas kernels  140 us (97%)
  local copies, waits for them, and re-layouts  2.3 us (2%)
    pallas_call x1, Pallas kernels, per_device(): pl.pallas_call(layer_kernel, out_shape=sds((TOK, 2048), BF), in_specs=[AN...  140 us

profile of v4, /device:TPU:6, one launch (start us, length us, event | category | flops | bytes accessed | tf_op | source)
XLA Modules:
  0.0 143.5 jit_solution(950646989929973093)
XLA Ops:
  0.0 0.8 fusion
  0.9 140.3 %layer.1 = bf16[256,2048]{1,0:T(8,128)(2,1)} custom-call(bf16[256,2048]{1,0:T(8,128)(2,1)} %bitcast.21, bf16[256,512]{1,0:T(8,128)(2,1)} %bitcast.23, bf16[256,512]{1,0:T(8,128)(2,1)} %bitcast.24, bf16[256,2048]{1,0:T(8,128)(2,1)} %bitcast.22, bf16[256,2048]{1,0:T(8,128)(2,1)} %w_hbm.1, bf16[2048,1024]{1,0:T(8,128)(2,1)} %bitcast.18, ...), custom_call_target="tpu_custom_call" | custom-call | tf_op jit(solution)/shard_map/layer/pallas_call | solution.py:483
  141.2 2.3 %copy.15 = bf16[1,256,2048]{2,1,0:T(8,128)(2,1)} copy(bf16[1,256,2048]{2,1,0:T(8,128)(2,1)} %bitcast.17) | data formatting | bytes 2097152
  (2 shorter events, 0.0 us)

commit v5 on v4

--- a/solution.py
+++ b/solution.py
@@ -83,8 +83,8 @@
     slot_ref[...] = jnp.sum(jnp.where(target == slots, token, 0.0), axis=0, keepdims=True).astype(jnp.int32)
 
 
-STEP_BLOCK = (3, 0, 1, 2, 0, 0, 1, 1, 0, 1, 2, 2, 2, 3, 3, 3)
-STEP_QUARTER = (0, 0, 0, 0, 1, 3, 1, 3, 2, 2, 1, 3, 2, 1, 3, 2)
+STEP_BLOCK = (3, 0, 0, 0, 1, 1, 1, 0, 1, 2, 2, 2, 2, 3, 3, 3)
+STEP_QUARTER = (0, 0, 1, 3, 0, 1, 3, 2, 2, 0, 1, 3, 2, 1, 3, 2)
 
 
 def step_entry(table, i):
@@ -247,26 +247,23 @@
         t, turn = step_entry(STEP_BLOCK, i), step_entry(STEP_QUARTER, i)
         a, quarter = lax.rem(z + 1 + t, ZN), lax.rem(x + ZN - turn, XN)
 
-        @pl.when((i > 0) & (i < 4))
+        @pl.when(i == 1)
+        def _():
+            forward(1)
+            forward(3)
+
+        @pl.when((i > 0) & (turn == 0))
         def _():
             remote(qs.at[a], qr.at[a], zqs.at[2 - t], zqr.at[2 - t], sp_of(a, x)).wait_recv()
 
-        @pl.when(i == 1)
-        def _():
-            forward(1)
-
-        @pl.when(i == 3)
-        def _():
-            forward(3)
-
-        @pl.when(i == 4)
+        @pl.when(i == 2)
         def _():
             forward(2)
             near[2][0].wait_recv()
             near[3][0].wait_recv()
             value_quarter(quarter)
 
-        @pl.when(i == 5)
+        @pl.when(i == 3)
         def _():
             near[0][1].wait_recv()
             near[1][1].wait_recv()
@@ -279,7 +276,7 @@
             near_w[1, 1].wait_recv()
             remote(shard(above, 1), shard(above, 1), w2s.at[1], w2r.at[1], {"dp": below}).start()
 
-        @pl.when(i == 8)
+        @pl.when(i == 7)
         def _():
             for d in range(4):
                 far_copy(d).wait_recv()

time: 145 us -> 163 us (1.12)
  Pallas kernels: 140 us -> 160 us
    pallas_call x1, Pallas kernels: 140 us -> 160 us  [per_device(): pl.pallas_call(layer_kernel, out_shape=sds((TOK, 2048), BF), in_specs=[AN...]
where the time goes in v5:
time: 163 us
  Pallas kernels  160 us (98%)
  local copies, waits for them, and re-layouts  2.3 us (1%)
    pallas_call x1, Pallas kernels, per_device(): pl.pallas_call(layer_kernel, out_shape=sds((TOK, 2048), BF), in_specs=[AN...  160 us

profile of v5, /device:TPU:6, one launch (start us, length us, event | category | flops | bytes accessed | tf_op | source)
XLA Modules:
  0.0 162.8 jit_solution(10470326213280954696)
XLA Ops:
  0.0 0.8 fusion
  0.9 159.6 %layer.1 = bf16[256,2048]{1,0:T(8,128)(2,1)} custom-call(bf16[256,2048]{1,0:T(8,128)(2,1)} %bitcast.21, bf16[256,512]{1,0:T(8,128)(2,1)} %bitcast.23, bf16[256,512]{1,0:T(8,128)(2,1)} %bitcast.24, bf16[256,2048]{1,0:T(8,128)(2,1)} %bitcast.22, bf16[256,2048]{1,0:T(8,128)(2,1)} %w_hbm.1, bf16[2048,1024]{1,0:T(8,128)(2,1)} %bitcast.18, ...), custom_call_target="tpu_custom_call" | custom-call | tf_op jit(solution)/shard_map/layer/pallas_call | solution.py:480
  160.5 2.3 %copy.15 = bf16[1,256,2048]{2,1,0:T(8,128)(2,1)} copy(bf16[1,256,2048]{2,1,0:T(8,128)(2,1)} %bitcast.17) | data formatting | bytes 2097152
  (2 shorter events, 0.0 us)
